TPU v7x, 256 devices: a 4x2x16 block of a 4x16x16 slice. The times are simulated.
256 devices in a mesh: grp: 2 (over y), ep: 32 (over z, core), tp: 4 (over x).
Axes of the slice: x: 4, y: 2, z: 16, core: 2. Of those that a mesh axis runs over, the one named last changes fastest.
The devices are a block of a 4x16x16 slice.
Arguments:
- queries: bfloat16 [16384, 2048], P(('grp', 'ep'), 'tp'), parts along dimension 0, may hold values from -8 to 8
- key_rows: bfloat16 [16384, 2048], P(('grp', 'ep'), 'tp'), parts along dimension 0, may hold values from -8 to 8
- value_rows: bfloat16 [16384, 2048], P(('grp', 'ep'), 'tp'), parts along dimension 0, may hold values from -6 to 6
- mix_lambda: float32 [32], P('tp'), may hold values from 0.3 to 0.8
- head_gain: float32 [64], replicated, may hold values from 0.1 to 1.9
- out_weight: bfloat16 [2048, 2048], P('tp'), may hold values from -0.125 to 0.125
- expert_in: bfloat16 [16384, 2048], P(('grp', 'ep', 'tp')), parts along dimension 0, may hold values from -6 to 6
- expert_gain: float32 [2048], replicated, may hold values from 0.1 to 1.9
- routes: int32 [16384, 2], P(('grp', 'ep', 'tp')), parts along dimension 0, may hold values from 0 to 31, all different within a row; in each aligned block of 64 rows (0 to 63, 64 to 127, ...) at most 5 rows name the same one
- route_logits: float32 [16384, 2], P(('grp', 'ep', 'tp')), parts along dimension 0, may hold values from -6 to 6
- gate_weight: bfloat16 [32, 2048, 2048], P('ep', None, 'tp'), may hold values from -1 to 1
- up_weight: bfloat16 [32, 2048, 2048], P('ep', None, 'tp'), may hold values from -1 to 1
- down_weight: bfloat16 [32, 2048, 2048], P('ep', 'tp'), may hold values from -0.125 to 0.125
Outputs:
- mixer_out: bfloat16 [16384, 2048], P(('grp', 'ep', 'tp')), parts along dimension 0
- expert_out: bfloat16 [16384, 2048], P(('grp', 'ep', 'tp')), parts along dimension 0
There are 2 independent parts, one for each index of `grp`. A program takes and returns all parts, laid end to end along the dimension named above; an argument that names none is the same for every part. Nothing has to cross between parts.
Inputs may be any that keep to these rules, and one draw needn't show every extreme that they name: `routes`: each row names 2 different experts; in each aligned block of 64 rows (the rows of one device) no expert is named by more than 5 rows, a bound that some block reaches.
All inputs are finite; a program needn't handle non-finite values.
Results may differ from a plain program's by a relative error of at most 0.014.
Values may be sent and summed in bfloat16 or wider, within the bound.
A program may use at most 128 MiB of HBM per device.

v0:
```python
import math

import jax
import jax.numpy as jnp
from jax import lax
from jax.sharding import Mesh
from jax.sharding import PartitionSpec as P

DQK = 32
DV = 64
EP = ("ep_0", "ep_1")
GRP_EP = ("grp", "ep_0", "ep_1")
GRP_EP_TP = ("grp", "ep_0", "ep_1", "tp")


HEAD_EPS = 0.0001
NORM_EPS = 0.1
POST_EPS = 1.0
CLAMP_LIMIT = 7.0
SIGMOID_SCALE = 1.702
OUT_SCALE = 0.8


def in_one_piece(arrays, axis, dim, along):
    ends, at = ([], 0)
    for a in arrays[:-1]:
        at += a.shape[along]
        ends.append(at)
    both = jnp.concatenate(arrays, axis=along)
    return tuple(jnp.split(lax.all_gather(both, axis, axis=dim, tiled=True), ends, axis=along))


def split_up(array, dim, count):
    dims = array.shape
    parts = array.reshape(*dims[:dim], count, dims[dim] // count, *dims[dim + 1 :])
    return jnp.moveaxis(parts, dim, 0)


def sent_and_summed(array, axis, dim):
    parts = split_up(array, dim, lax.axis_size(axis))
    arrived = lax.all_to_all(parts, axis, split_axis=0, concat_axis=0, tiled=True)
    return arrived.astype(jnp.float32).sum(axis=0)


def from_everyone(array, axis):
    count = lax.axis_size(axis)
    return lax.all_to_all(
        jnp.broadcast_to(array[None], (count, *array.shape)), axis, 0, 0, tiled=True
    )


def in_order(parts, dim):
    dims = list(parts.shape[1:])
    dims[dim] *= parts.shape[0]
    return jnp.moveaxis(parts, 0, dim).reshape(dims)


def gather_directly(array, axis, dim):
    parts = from_everyone(array, axis)
    return in_order(parts, dim)


def exchange_in_order(parts, axes, order):
    inside = parts.shape[1:]
    whole = parts.reshape(*(lax.axis_size(a) for a in axes), *inside)
    for k in order:
        whole = lax.all_to_all(whole, axes[k], k, k, tiled=True)
    return whole.reshape(-1, *inside)


def two_step_exchange(array, groups, order, split_dim, concat_dim):
    count = lax.axis_size(groups[0]) * lax.axis_size(groups[1])
    parts = split_up(array, split_dim, count)
    return in_order(exchange_in_order(parts, groups, order), concat_dim)


def local(
    queries,
    key_rows,
    value_rows,
    mix_lambda,
    head_gain,
    out_weight,
    expert_in,
    expert_gain,
    routes,
    route_logits,
    gate_weight,
    up_weight,
    down_weight,
):
    row_count = queries.shape[0]
    local_heads = queries.shape[1] // (2 * DQK)
    query_heads = queries.reshape(row_count, local_heads, 2, DQK)
    scale_factor = DQK ** (-0.5)
    start_state = (
        jnp.full((local_heads, 2, row_count), -jnp.inf, jnp.float32),
        jnp.zeros((local_heads, 2, row_count), jnp.float32),
        jnp.zeros((local_heads, 2, row_count, DV), jnp.float32),
    )
    key_piece, value_piece = in_one_piece((key_rows, value_rows), EP, 0, 1)
    piece_len = key_piece.shape[0]
    block_len = math.gcd(piece_len, 512)

    def step_block(block_index, carried):
        running_max, running_sum, running_acc = carried
        key_block = lax.dynamic_slice_in_dim(key_piece, block_index * block_len, block_len, 0)
        key_block = key_block.reshape(block_len, local_heads, 2, DQK)
        value_block = lax.dynamic_slice_in_dim(value_piece, block_index * block_len, block_len, 0)
        value_block = value_block.reshape(block_len, local_heads, DV)
        scores = (
            jnp.einsum(
                "qhmd,khmd->hmqk", query_heads, key_block, preferred_element_type=jnp.float32
            )
            * scale_factor
        )
        new_max = jnp.maximum(running_max, jnp.max(scores, axis=-1))
        shrink = jnp.exp(running_max - new_max)
        exponents = jnp.exp(scores - new_max[..., None])
        running_sum = running_sum * shrink + jnp.sum(exponents, axis=-1)
        running_acc = running_acc * shrink[..., None] + jnp.einsum(
            "hmqk,khd->hmqd",
            exponents.astype(jnp.bfloat16),
            value_block,
            preferred_element_type=jnp.float32,
        )
        return (new_max, running_sum, running_acc)

    final_max, final_sum, final_acc = lax.fori_loop(
        0, piece_len // block_len, step_block, start_state
    )
    attended = final_acc / final_sum[..., None]
    differ = attended[:, 0] - mix_lambda[:, None, None] * attended[:, 1]
    normed_heads = differ * lax.rsqrt(jnp.mean(differ * differ, axis=-1, keepdims=True) + HEAD_EPS)
    normed_heads = (normed_heads * head_gain * OUT_SCALE).astype(jnp.bfloat16)
    head_rows = jnp.transpose(normed_heads, (1, 0, 2)).reshape(row_count, local_heads * DV)
    selected = head_rows
    mixer_out = sent_and_summed(
        jnp.dot(selected, out_weight, preferred_element_type=jnp.float32).astype(jnp.bfloat16),
        "tp",
        0,
    ).astype(jnp.bfloat16)
    tokens_here = expert_in.shape[0]
    top_count = routes.shape[1]
    experts_all = lax.axis_size(EP) * gate_weight.shape[0]
    capacity = (5 * tokens_here * top_count + 4 * experts_all - 1) // (4 * experts_all)
    inputs_wide = expert_in.astype(jnp.float32)
    normed = inputs_wide * lax.rsqrt(
        jnp.mean(inputs_wide * inputs_wide, axis=-1, keepdims=True) + NORM_EPS
    )
    normed = (normed * expert_gain).astype(jnp.bfloat16)
    flat_routes = routes.reshape(-1)
    expert_ids = jnp.arange(experts_all, dtype=jnp.int32)
    onehot_table = (flat_routes[:, None] == expert_ids[None, :]).astype(jnp.int32)
    ranks = jnp.cumsum(onehot_table, axis=0) - onehot_table
    slot_pos = jnp.sum(ranks * onehot_table, axis=1)
    slot_ids = flat_routes * capacity + slot_pos
    slot_grid = jnp.arange(experts_all * capacity, dtype=jnp.int32)
    placing = (slot_grid[:, None] == slot_ids[None, :]).astype(jnp.bfloat16)
    placing = placing.reshape(experts_all * capacity, tokens_here, top_count).sum(axis=2)
    dispatch = jnp.dot(placing, normed, preferred_element_type=jnp.float32).astype(jnp.bfloat16)
    dispatch = dispatch.reshape(experts_all, capacity, -1)
    gate_local = gate_weight[0]
    up_local = up_weight[0]
    down_local = down_weight[0]
    arrived = two_step_exchange(dispatch, ("ep_0", "ep_1"), (1, 0), 0, 0)
    sources, slot_count, channels = arrived.shape
    flat_rows = arrived.reshape(sources * slot_count, channels)
    pieces = gather_directly(flat_rows, "tp", 0)
    gate_pre = jnp.dot(pieces, gate_local, preferred_element_type=jnp.float32)
    up_pre = jnp.dot(pieces, up_local, preferred_element_type=jnp.float32)
    clipped_gate = jnp.minimum(gate_pre, CLAMP_LIMIT)
    clipped_up = jnp.clip(up_pre, -CLAMP_LIMIT, CLAMP_LIMIT)
    act_rows = (
        clipped_gate * jax.nn.sigmoid(SIGMOID_SCALE * clipped_gate) * (clipped_up + 1.0)
    ).astype(jnp.bfloat16)
    selected = act_rows
    summed = sent_and_summed(
        jnp.dot(selected, down_local, preferred_element_type=jnp.float32).astype(jnp.bfloat16),
        "tp",
        0,
    )
    returned = summed.astype(jnp.bfloat16).reshape(sources, slot_count, channels)
    arrived_back = lax.all_to_all(returned, EP, split_axis=0, concat_axis=0, tiled=True)
    flat_back = arrived_back.reshape(experts_all * capacity, -1)
    picked = (
        jnp.take(flat_back, slot_ids, axis=0)
        .astype(jnp.float32)
        .reshape(tokens_here, top_count, -1)
    )
    route_weight = 1.0 / jnp.sum(
        jnp.exp(route_logits[:, None, :] - route_logits[:, :, None]), axis=-1
    )
    combined = jnp.sum(route_weight[..., None] * picked, axis=1)
    expert_out = combined * lax.rsqrt(
        jnp.mean(combined * combined, axis=-1, keepdims=True) + POST_EPS
    )
    return (mixer_out, expert_out.astype(jnp.bfloat16))


def solution(mesh):
    finer = Mesh(
        mesh.devices.reshape(mesh.shape["grp"], 16, 2, mesh.shape["tp"]),
        ("grp", "ep_0", "ep_1", "tp"),
    )
    return jax.shard_map(
        local,
        mesh=finer,
        in_specs=(
            P(GRP_EP, "tp"),
            P(GRP_EP, "tp"),
            P(GRP_EP, "tp"),
            P("tp"),
            P(),
            P("tp", None),
            P(GRP_EP_TP, None),
            P(),
            P(GRP_EP_TP, None),
            P(GRP_EP_TP, None),
            P(EP, None, "tp"),
            P(EP, None, "tp"),
            P(EP, "tp", None),
        ),
        out_specs=(P(GRP_EP_TP, None), P(GRP_EP_TP, None)),
        check_vma=False,
    )
```

profile of v0, /device:TPU:33, one launch (start us, length us, event | category | flops | bytes accessed | tf_op | source)
XLA Modules:
  0.0 499.7 jit_solution(12308034031106010059)
XLA Ops:
  14.8 24.3 %all_to_all.30 = bf16[16,2,1,5,2048]{4,0,3,2,1:T(8,128)(2,1)S(1)} all-to-all(bf16[16,2,1,5,2048]{4,0,3,2,1:T(8,128)(2,1)S(1)} %copy.66), channel_id=1, replica_groups=mesh['grp'=2,'ep_0'=16,'ep_1'=2,'tp'=4] {'ep_1'}, dimensions={1} | all-to-all | bytes 1310720 | tf_op jit(solution)/shard_map/all_to_all | solution.py:67
  39.8 44.4 %all_to_all.31 = bf16[16,2,1,5,2048]{4,1,3,2,0:T(2,128)(2,1)S(1)} all-to-all(bf16[16,2,1,5,2048]{4,1,3,2,0:T(2,128)(2,1)S(1)} %copy.67), channel_id=1, replica_groups=mesh['grp'=2,'ep_0'=16,'ep_1'=2,'tp'=4] {'ep_0'}, dimensions={0} | all-to-all | bytes 1310720 | tf_op jit(solution)/shard_map/all_to_all | solution.py:67
  87.0 33.0 %all_to_all.32 = bf16[4,160,2048]{2,1,0:T(8,128)(2,1)S(1)} all-to-all(bf16[4,160,2048]{2,1,0:T(8,128)(2,1)S(1)} %broadcast_in_dim.50), channel_id=1, replica_groups=mesh['grp'=2,'ep_0'=16,'ep_1'=2,'tp'=4] {'tp'}, dimensions={0} | all-to-all | bytes 5242880 | tf_op jit(solution)/shard_map/all_to_all | solution.py:47
  123.0 7.0 %convolution_convert_fusion = bf16[640,2048]{1,0:T(8,128)(2,1)} fusion(bf16[1,512,2048]{2,1,0:T(8,128)(2,1)S(1)} %copy-done, bf16[640,2048]{1,0:T(8,128)(2,1)} %bitcast.103, bf16[1,2048,512]{2,1,0:T(8,128)(2,1)} %param.26, f32[640,512]{1,0:T(8,128)S(1)} %fusion.18), kind=kOutput, calls=%fused_computation.19 | convolution fusion | flops 2688614400 | bytes 10747904 | tf_op jit(solution)/shard_map/dot_general | solution.py:179
  130.0 32.8 %all_to_all.33 = bf16[4,160,2048]{2,1,0:T(8,128)(2,1)} all-to-all(bf16[4,160,2048]{2,1,0:T(8,128)(2,1)} %bitcast.104), channel_id=1, replica_groups=mesh['grp'=2,'ep_0'=16,'ep_1'=2,'tp'=4] {'tp'}, dimensions={0} | all-to-all | bytes 5242880 | tf_op jit(solution)/shard_map/all_to_all | solution.py:41
  166.5 15.0 %all-to-all-start.5 = ((bf16[32,5,2048]{2,1,0:T(8,128)(2,1)}), bf16[32,5,2048]{2,1,0:T(8,128)(2,1)S(1)}, u32[]{:S(2)}, u32[]{:S(2)}) async-start(bf16[32,5,2048]{2,1,0:T(8,128)(2,1)} %reshape.144), calls=%async_computation.5 | async-start | bytes 2097152 | tf_op jit(solution)/shard_map/all_to_all | solution.py:184
  182.2 54.8 %all-to-all-done.5 = bf16[32,5,2048]{2,1,0:T(8,128)(2,1)S(1)} async-done(((bf16[32,5,2048]{2,1,0:T(8,128)(2,1)}), bf16[32,5,2048]{2,1,0:T(8,128)(2,1)S(1)}, u32[]{:S(2)}, u32[]{:S(2)}) %all-to-all-start.5) | async-done | bytes 655392 | tf_op jit(solution)/shard_map/all_to_all | solution.py:184
  241.0 11.6 %fusion.57 = (bf16[8192,512]{0,1:T(8,128)(2,1)}, bf16[8192,512]{0,1:T(8,128)(2,1)}) fusion(bf16[8192,1024]{0,1:T(8,128)(2,1)} %all-gather.2.cloned.1.call-done), kind=kLoop, calls=%fused_computation.78 | loop fusion | bytes 33554432 | tf_op jit(solution)/shard_map/split | solution.py:30
  252.6 215.7 %while.18 = (s32[]{:T(128)}, f32[8,2,256]{2,1,0:T(2,128)S(1)}, f32[8,2,256]{2,1,0:T(2,128)S(1)}, f32[8,2,256,64]{2,3,1,0:T(8,128)S(1)}, bf16[8192,512]{0,1:T(8,1...) while((s32[]{:T(128)}, f32[8,2,256]{2,1,0:T(2,128)S(1)}, ...), condition=%wide.region_3.0_spmd.clone, body=%wide.region_0.0_spmd.clone.sunk | while | flops 420237312 | bytes 64487620 | solution.py:129
  253.9 4.5 bitcast_reduce_fusion.2
  258.4 4.9 fusion.79
  267.4 4.5 bitcast_reduce_fusion.2
  271.9 4.9 fusion.79
  285.4 4.9 fusion.79
  298.9 4.9 fusion.79
  307.8 4.5 bitcast_reduce_fusion.2
  312.4 4.9 fusion.79
  321.3 4.5 bitcast_reduce_fusion.2
  325.8 4.9 fusion.79
  339.3 4.9 fusion.79
  352.8 4.9 fusion.79
  361.7 4.5 bitcast_reduce_fusion.2
  366.3 4.9 fusion.79
  375.2 4.5 bitcast_reduce_fusion.2
  379.8 4.9 fusion.79
  393.3 4.9 fusion.79
  406.7 4.9 fusion.79
  420.2 4.9 fusion.79
  433.7 4.9 fusion.79
  447.2 4.9 fusion.79
  460.7 4.9 fusion.79
  477.0 13.7 %all-to-all-done = bf16[4,64,2048]{2,1,0:T(8,128)(2,1)} async-done(((bf16[4,64,2048]{2,1,0:T(8,128)(2,1)}), bf16[4,64,2048]{2,1,0:T(8,128)(2,1)}, u32[]{:S(2)}, u32[]{:S(2)}) %all-to-all-start) | async-done | bytes 1048608 | tf_op jit(solution)/shard_map/all_to_all | solution.py:41
  (200 shorter events, 141.8 us)
Async XLA Ops:
  7.2 115.9 %copy-start = (bf16[1,512,2048]{2,1,0:T(8,128)(2,1)S(1)}, bf16[1,512,2048]{2,1,0:T(8,128)(2,1)}, u32[]{:S(2)}) copy-start(bf16[1,512,2048]{2,1,0:T(8,128)(2,1)} %param.27) | copy-start | bytes 6291460
  7.2 3.3 copy-start.7
  7.2 4.3 copy-start.5
  7.2 4.5 copy-start.8
  7.2 233.8 %all-gather.2.cloned.1.call-start = ((), (), s32[]{:S(2)}) async-start(), calls=%async_computation.6 | async-start | bytes 17301504 | tf_op jit(solution)/shard_map/all_gather | solution.py:30
  87.0 34.5 %copy-start.12 = (bf16[1,2048,512]{2,1,0:T(8,128)(2,1)S(1)}, bf16[1,2048,512]{2,1,0:T(8,128)(2,1)}, u32[]{:S(2)}) copy-start(bf16[1,2048,512]{2,1,0:T(8,128)(2,1)} %param.25) | copy-start | bytes 6291460
  120.0 1.5 copy-start.3
  165.2 16.7 %copy-start.9 = (f32[64,2]{0,1:T(2,128)S(1)}, f32[64,2]{0,1:T(2,128)}, u32[]{:S(2)}) copy-start(f32[64,2]{0,1:T(2,128)} %param.24) | copy-start | bytes 1540
  165.2 16.8 %copy-start.6 = (bf16[256,512]{1,0:T(8,128)(2,1)S(1)}, bf16[256,512]{1,0:T(8,128)(2,1)}, u32[]{:S(2)}) copy-start(bf16[256,512]{1,0:T(8,128)(2,1)} %param.15) | copy-start | bytes 786436
  166.5 70.4 %all-to-all-start.5 = ((bf16[32,5,2048]{2,1,0:T(8,128)(2,1)}), bf16[32,5,2048]{2,1,0:T(8,128)(2,1)S(1)}, u32[]{:S(2)}, u32[]{:S(2)}) async-start(bf16[32,5,2048]{2,1,0:T(8,128)(2,1)} %reshape.144), calls=%async_computation.5 | async-start | bytes 2097152 | tf_op jit(solution)/shard_map/all_to_all | solution.py:184
  252.6 215.9 %copy-start.10 = (f32[8]{0:T(128)S(1)}, f32[8]{0:T(128)}, u32[]{:S(2)}) copy-start(f32[8]{0:T(128)} %param.18) | copy-start | bytes 100
  258.4 5.8 %copy-start.2 = (f32[8,2,512,256]{3,2,1,0:T(8,128)S(1)}, f32[8,2,512,256]{3,2,1,0:T(8,128)}, u32[]{:S(2)}) copy-start(f32[8,2,512,256]{3,2,1,0:T(8,128)} %get-tuple-element.228) | copy-start | bytes 25165828 | tf_op jit(solution)/shard_map/while
  271.9 5.8 %copy-start.2 = (f32[8,2,512,256]{3,2,1,0:T(8,128)S(1)}, f32[8,2,512,256]{3,2,1,0:T(8,128)}, u32[]{:S(2)}) copy-start(f32[8,2,512,256]{3,2,1,0:T(8,128)} %get-tuple-element.228) | copy-start | bytes 25165828 | tf_op jit(solution)/shard_map/while
  285.4 5.8 %copy-start.2 = (f32[8,2,512,256]{3,2,1,0:T(8,128)S(1)}, f32[8,2,512,256]{3,2,1,0:T(8,128)}, u32[]{:S(2)}) copy-start(f32[8,2,512,256]{3,2,1,0:T(8,128)} %get-tuple-element.228) | copy-start | bytes 25165828 | tf_op jit(solution)/shard_map/while
  298.9 5.8 %copy-start.2 = (f32[8,2,512,256]{3,2,1,0:T(8,128)S(1)}, f32[8,2,512,256]{3,2,1,0:T(8,128)}, u32[]{:S(2)}) copy-start(f32[8,2,512,256]{3,2,1,0:T(8,128)} %get-tuple-element.228) | copy-start | bytes 25165828 | tf_op jit(solution)/shard_map/while
  312.4 5.8 %copy-start.2 = (f32[8,2,512,256]{3,2,1,0:T(8,128)S(1)}, f32[8,2,512,256]{3,2,1,0:T(8,128)}, u32[]{:S(2)}) copy-start(f32[8,2,512,256]{3,2,1,0:T(8,128)} %get-tuple-element.228) | copy-start | bytes 25165828 | tf_op jit(solution)/shard_map/while
  325.8 5.8 %copy-start.2 = (f32[8,2,512,256]{3,2,1,0:T(8,128)S(1)}, f32[8,2,512,256]{3,2,1,0:T(8,128)}, u32[]{:S(2)}) copy-start(f32[8,2,512,256]{3,2,1,0:T(8,128)} %get-tuple-element.228) | copy-start | bytes 25165828 | tf_op jit(solution)/shard_map/while
  339.3 5.8 %copy-start.2 = (f32[8,2,512,256]{3,2,1,0:T(8,128)S(1)}, f32[8,2,512,256]{3,2,1,0:T(8,128)}, u32[]{:S(2)}) copy-start(f32[8,2,512,256]{3,2,1,0:T(8,128)} %get-tuple-element.228) | copy-start | bytes 25165828 | tf_op jit(solution)/shard_map/while
  352.8 5.8 %copy-start.2 = (f32[8,2,512,256]{3,2,1,0:T(8,128)S(1)}, f32[8,2,512,256]{3,2,1,0:T(8,128)}, u32[]{:S(2)}) copy-start(f32[8,2,512,256]{3,2,1,0:T(8,128)} %get-tuple-element.228) | copy-start | bytes 25165828 | tf_op jit(solution)/shard_map/while
  366.3 5.8 %copy-start.2 = (f32[8,2,512,256]{3,2,1,0:T(8,128)S(1)}, f32[8,2,512,256]{3,2,1,0:T(8,128)}, u32[]{:S(2)}) copy-start(f32[8,2,512,256]{3,2,1,0:T(8,128)} %get-tuple-element.228) | copy-start | bytes 25165828 | tf_op jit(solution)/shard_map/while
  379.8 5.8 %copy-start.2 = (f32[8,2,512,256]{3,2,1,0:T(8,128)S(1)}, f32[8,2,512,256]{3,2,1,0:T(8,128)}, u32[]{:S(2)}) copy-start(f32[8,2,512,256]{3,2,1,0:T(8,128)} %get-tuple-element.228) | copy-start | bytes 25165828 | tf_op jit(solution)/shard_map/while
  393.2 5.8 %copy-start.2 = (f32[8,2,512,256]{3,2,1,0:T(8,128)S(1)}, f32[8,2,512,256]{3,2,1,0:T(8,128)}, u32[]{:S(2)}) copy-start(f32[8,2,512,256]{3,2,1,0:T(8,128)} %get-tuple-element.228) | copy-start | bytes 25165828 | tf_op jit(solution)/shard_map/while
  406.7 5.8 %copy-start.2 = (f32[8,2,512,256]{3,2,1,0:T(8,128)S(1)}, f32[8,2,512,256]{3,2,1,0:T(8,128)}, u32[]{:S(2)}) copy-start(f32[8,2,512,256]{3,2,1,0:T(8,128)} %get-tuple-element.228) | copy-start | bytes 25165828 | tf_op jit(solution)/shard_map/while
  420.2 5.8 %copy-start.2 = (f32[8,2,512,256]{3,2,1,0:T(8,128)S(1)}, f32[8,2,512,256]{3,2,1,0:T(8,128)}, u32[]{:S(2)}) copy-start(f32[8,2,512,256]{3,2,1,0:T(8,128)} %get-tuple-element.228) | copy-start | bytes 25165828 | tf_op jit(solution)/shard_map/while
  433.7 5.8 %copy-start.2 = (f32[8,2,512,256]{3,2,1,0:T(8,128)S(1)}, f32[8,2,512,256]{3,2,1,0:T(8,128)}, u32[]{:S(2)}) copy-start(f32[8,2,512,256]{3,2,1,0:T(8,128)} %get-tuple-element.228) | copy-start | bytes 25165828 | tf_op jit(solution)/shard_map/while
  447.2 5.8 %copy-start.2 = (f32[8,2,512,256]{3,2,1,0:T(8,128)S(1)}, f32[8,2,512,256]{3,2,1,0:T(8,128)}, u32[]{:S(2)}) copy-start(f32[8,2,512,256]{3,2,1,0:T(8,128)} %get-tuple-element.228) | copy-start | bytes 25165828 | tf_op jit(solution)/shard_map/while
  460.7 5.8 %copy-start.2 = (f32[8,2,512,256]{3,2,1,0:T(8,128)S(1)}, f32[8,2,512,256]{3,2,1,0:T(8,128)}, u32[]{:S(2)}) copy-start(f32[8,2,512,256]{3,2,1,0:T(8,128)} %get-tuple-element.228) | copy-start | bytes 25165828 | tf_op jit(solution)/shard_map/while
  468.3 0.7 copy-start.11
  468.3 1.6 copy-start.4
  469.9 22.9 %copy-start.1 = (bf16[1,512,2048]{2,1,0:T(8,128)(2,1)S(1)}, bf16[1,512,2048]{2,1,0:T(8,128)(2,1)}, u32[]{:S(2)}) copy-start(bf16[1,512,2048]{2,1,0:T(8,128)(2,1)} %param.27) | copy-start | bytes 6291460
  471.7 19.0 %all-to-all-start = ((bf16[4,64,2048]{2,1,0:T(8,128)(2,1)}), bf16[4,64,2048]{2,1,0:T(8,128)(2,1)}, u32[]{:S(2)}, u32[]{:S(2)}) async-start(bf16[4,64,2048]{2,1,0:T(8,128)(2,1)} %bitcast.101), calls=%async_computation | async-start | bytes 2097152 | tf_op jit(solution)/shard_map/all_to_all | solution.py:41
Sparse Core Ops, SparseCore 0:
  10.6 171.6 all-gather.1
where the time goes:
time: 501 us; the launch traced here: 500 us
  blocking collectives  134 us (27%)
  matrix products  114 us (23%)
  other arithmetic  89.7 us (18%)
  waiting for transfers between devices  68.5 us (14%)
  local copies, waits for them, and re-layouts  58.8 us (12%)
  starting transfers between devices  19.4 us (4%)
  between operations  14.4 us (3%)
    reduce_sum x16, other arithmetic, step_block(): running_sum = running_sum * shrink + jnp.sum(exponents, axis=-1)  78.8 us
    dot_general x16, matrix products, step_block(): jnp.einsum('qhmd,khmd->hmqk', query_heads, key_block, preferred_element_t...  72.7 us
    all_to_all x2, blocking collectives, exchange_in_order(): whole = lax.all_to_all(whole, axes[k], k, k, tiled=True)  68.7 us
    all_to_all x1, waiting for transfers between devices, local(): lax.all_to_all(returned, EP, split_axis=0, concat_axis=0, tiled=True)  54.8 us
    all_to_all x1, blocking collectives, from_everyone(): lax.all_to_all(jnp.broadcast_to(array[None], (count, *array.shape)), axis...  33 us
    all_to_all x1, blocking collectives, sent_and_summed(): lax.all_to_all(parts, axis, split_axis=0, concat_axis=0, tiled=True)  32.8 us
    dot_general x16, matrix products, step_block(): jnp.einsum('hmqk,khd->hmqd', exponents.astype(jnp.bfloat16), value_block,...  29.3 us
    dynamic_slice x16, local copies, waits for them, and re-layouts, step_block(): lax.dynamic_slice_in_dim(value_piece, block_index * block_len, block_len, 0)  20.5 us
  transfers between devices with their start and end apart: 3, of which 2 were waited for; matrix products, arithmetic and copies ran while one was open for 5% of the time, Pallas kernels for 0%

commit v1 on v0

v1 whole, which is shorter than its diff:
```python
import functools
import math

import jax
import jax.numpy as jnp
from jax import lax
from jax.experimental import pallas as pl
from jax.experimental.pallas import tpu as pltpu
from jax.sharding import PartitionSpec as P

DQK = 32
DV = 64
HEAD_EPS = 0.0001
NORM_EPS = 0.1
POST_EPS = 1.0
CLAMP_LIMIT = 7.0
SIGMOID_SCALE = 1.702
OUT_SCALE = 0.8
CEXP = DQK ** -0.5 * math.log2(math.e)
LANES = 128
GROUP = 256
ONES = 16
LOOK = 2
MESH = pl.DeviceIdType.MESH
F32, BF16 = jnp.float32, jnp.bfloat16
K, V = 0, 1
R, L = 0, 1


def dot(a, b):
    return jnp.dot(a, b, preferred_element_type=F32)


def kernel(
    n_ep, n_tp, cap, stages,
    q_ref, k_ref, v_ref, lam_ref, gain_ref, x_ref, eg_ref, routes_ref, logit_ref,
    ow_hbm, gw_hbm, uw_hbm, dw_hbm,
    mix_ref, eo_ref,
    kbuf, vbuf, q_mask, m_ref, acc_ref,
    gw, uw, dw, ow,
    wide, packed, landed, xrows, act, part, precv, returned, comb, hr_ref, mp, mrecv,
    wsem, d_send, d_recv, r_send, r_recv, b_send, b_recv,
    x_send, x_recv, p_send, p_recv, e_send, e_recv, m_send, m_recv,
):
    ep, tp = lax.axis_index("ep"), lax.axis_index("tp")
    n_z = n_ep // 2
    half = n_z // 2
    z, core = ep // 2, lax.rem(ep, 2)
    sibling = 2 * z + 1 - core
    rows = q_ref.shape[0]
    heads = q_ref.shape[1] // (2 * DQK)
    maps = 2 * heads
    tokens, width = x_ref.shape
    n_lane = width // LANES
    slots = n_ep * cap
    fe = gw.shape[1]

    weight_copies = [
        pltpu.make_async_copy(src, dst, wsem.at[i])
        for i, (src, dst) in enumerate(((gw_hbm, gw), (uw_hbm, uw), (dw_hbm, dw), (ow_hbm, ow)))
    ]
    for copy in weight_copies:
        copy.start()

    barrier = pltpu.get_barrier_semaphore()

    def greet_ep(d, _):
        pl.semaphore_signal(barrier, inc=1, device_id={"ep": lax.rem(ep + d, n_ep)}, device_id_type=MESH)
        return 0

    def greet_tp(d, _):
        pl.semaphore_signal(barrier, inc=1, device_id={"tp": lax.rem(tp + d, n_tp)}, device_id_type=MESH)
        return 0

    lax.fori_loop(1, n_ep, greet_ep, 0)
    lax.fori_loop(1, n_tp, greet_tp, 0)

    routes = routes_ref[...].astype(F32)
    first, second = routes[:, 0:1], routes[:, 1:2]
    experts = lax.broadcasted_iota(jnp.int32, (tokens, n_ep), 1).astype(F32)
    is_first = (first == experts).astype(F32)
    is_second = (second == experts).astype(F32)
    earlier = (
        lax.broadcasted_iota(jnp.int32, (tokens, tokens), 0)
        > lax.broadcasted_iota(jnp.int32, (tokens, tokens), 1)
    ).astype(BF16)
    ahead = dot(earlier, (is_first + is_second).astype(BF16))
    slot_first = first * cap + jnp.sum(ahead * is_first, axis=1, keepdims=True)
    slot_second = second * cap + jnp.sum(ahead * is_second, axis=1, keepdims=True)

    def picks(slot, count):
        grid = lax.broadcasted_iota(jnp.int32, (tokens, count), 1).astype(F32)
        return (slot == grid).astype(BF16)

    x = x_ref[...].astype(F32)
    normed = x * lax.rsqrt(jnp.mean(x * x, axis=-1, keepdims=True) + NORM_EPS)
    normed = (normed * eg_ref[...]).astype(BF16)
    padded = -(-slots // LANES) * LANES
    placing = (picks(slot_first, padded) + picks(slot_second, padded)).astype(BF16)

    def to_tiles(j, columns):
        wide[pl.ds(j, slots, stride=n_lane), :] = columns

    step_cols = min(width, 512)
    for c0 in range(0, width, step_cols):
        placed = lax.dot_general(
            placing, normed[:, c0 : c0 + step_cols], (((0,), (0,)), ((), ())),
            preferred_element_type=F32,
        )
        for c1 in range(0, step_cols, LANES):
            to_tiles((c0 + c1) // LANES, placed[:slots, c1 : c1 + LANES])

    def pack_tiles(dst):
        def one(i, _):
            block = wide[pl.ds(pl.multiple_of(i * cap * n_lane, n_lane), cap * n_lane), :]
            dst[pl.ds(i * cap, cap)] = block.reshape(cap, n_lane, LANES).astype(BF16)
            return 0

        lax.fori_loop(0, n_ep, one, 0)

    def unpack_tiles(src):
        def one(i, _):
            block = src[pl.ds(i * cap, cap)].astype(F32)
            wide[pl.ds(pl.multiple_of(i * cap * n_lane, n_lane), cap * n_lane), :] = block.reshape(cap * n_lane, LANES)
            return 0

        lax.fori_loop(0, n_ep, one, 0)

    pack_tiles(packed)

    kbuf[ep] = k_ref[...]
    vbuf[ep] = v_ref[...].astype(F32).T.astype(BF16)
    q_cols = q_ref[...].astype(F32).T
    row_map = lax.broadcasted_iota(jnp.int32, (GROUP, rows), 0) // DQK
    per_group = GROUP // DQK
    for hm in range(maps):
        g = hm // per_group
        block = q_cols[GROUP * g : GROUP * g + GROUP]
        q_mask[hm] = jnp.where(row_map == hm % per_group, block, 0.0).astype(BF16)
        m_ref[hm] = jnp.full((1, rows), -1e30, F32)
        acc_ref[hm] = jnp.zeros((DV + ONES, rows), F32)

    pl.semaphore_wait(barrier, n_ep - 1 + n_tp - 1)

    def slot_copy(src, dst, send, recv, d):
        to = lax.rem(ep + d, n_ep)
        return pltpu.make_async_remote_copy(
            src_ref=src.at[pl.ds(to * cap, cap)],
            dst_ref=dst.at[pl.ds(ep * cap, cap)],
            send_sem=send.at[d], recv_sem=recv.at[d],
            device_id={"ep": to}, device_id_type=MESH,
        )

    def slot_arrival(dst, send, recv, d):
        source = lax.rem(ep + n_ep - d, n_ep)
        here = dst.at[pl.ds(source * cap, cap)]
        return pltpu.make_async_remote_copy(
            src_ref=here, dst_ref=here, send_sem=send.at[d], recv_sem=recv.at[d],
            device_id={"ep": source}, device_id_type=MESH,
        )

    def send_slots(src, dst, send, recv):
        def pair(i, _):
            slot_copy(src, dst, send, recv, i).start()
            slot_copy(src, dst, send, recv, n_ep - i).start()
            return 0

        lax.fori_loop(1, n_ep // 2, pair, 0)
        slot_copy(src, dst, send, recv, n_ep // 2).start()
        dst[pl.ds(ep * cap, cap)] = src[pl.ds(ep * cap, cap)]

    def take_slots(dst, send, recv):
        def one(d, _):
            slot_arrival(dst, send, recv, d).wait_recv()
            return 0

        lax.fori_loop(1, n_ep, one, 0)

    def flush_slots(src, dst, send, recv):
        def one(d, _):
            slot_copy(src, dst, send, recv, d).wait_send()
            return 0

        lax.fori_loop(1, n_ep, one, 0)

    send_slots(packed, landed, d_send, d_recv)

    bufs = (kbuf, vbuf)
    limits = ((half, half - 1), (half - 1, half))

    def block_at(direction, s):
        return lax.rem(z + n_z - s, n_z) if direction == R else lax.rem(z + s, n_z)

    def ring_copy(a, direction, s):
        there = bufs[a].at[2 * block_at(direction, s - 1) + core]
        to = lax.rem(ep + 2, n_ep) if direction == R else lax.rem(ep + n_ep - 2, n_ep)
        return pltpu.make_async_remote_copy(
            src_ref=there, dst_ref=there,
            send_sem=r_send.at[a, direction, s], recv_sem=r_recv.at[a, direction, s],
            device_id={"ep": to}, device_id_type=MESH,
        )

    def ring_arrival(a, direction, s):
        here = bufs[a].at[2 * block_at(direction, s) + core]
        source = lax.rem(ep + n_ep - 2, n_ep) if direction == R else lax.rem(ep + 2, n_ep)
        return pltpu.make_async_remote_copy(
            src_ref=here, dst_ref=here,
            send_sem=r_send.at[a, direction, s], recv_sem=r_recv.at[a, direction, s],
            device_id={"ep": source}, device_id_type=MESH,
        )

    def across(a, direction, s, owner):
        here = bufs[a].at[2 * block_at(direction, s) + owner]
        return pltpu.make_async_remote_copy(
            src_ref=here, dst_ref=here,
            send_sem=b_send.at[a, direction, s], recv_sem=b_recv.at[a, direction, s],
            device_id={"ep": sibling}, device_id_type=MESH,
        )

    for a in (K, V):
        for direction in (R, L):
            ring_copy(a, direction, 1).start()
        across(a, R, 0, core).start()

    def hop(a, direction, s):
        limit = limits[a][direction]

        @pl.when(s <= limit)
        def _():
            ring_arrival(a, direction, s).wait_recv()

            @pl.when(s < limit)
            def _():
                ring_copy(a, direction, s + 1).start()

            across(a, direction, s, core).start()

    def absorb_chip(chip):
        ones = jnp.ones((ONES, 2 * rows), BF16)

        def score(hm):
            c0 = GROUP * (hm // per_group)
            keys = jnp.concatenate([kbuf[2 * chip + b, :, c0 : c0 + GROUP] for b in (0, 1)], axis=0)
            return dot(keys, q_mask[hm])

        def values(h):
            cols = [vbuf[2 * chip + b, DV * h : DV * h + DV, :] for b in (0, 1)]
            return jnp.concatenate([jnp.concatenate(cols, axis=1), ones], axis=0)

        pending = [score(i) for i in range(min(LOOK, maps))]
        for hm in range(maps):
            if hm + LOOK < maps:
                pending.append(score(hm + LOOK))
            s = pending.pop(0)
            m_old = m_ref[hm]
            m_new = jnp.maximum(m_old, jnp.max(s, axis=0, keepdims=True))
            weights = jnp.exp2(s * CEXP - m_new * CEXP).astype(BF16)
            shrink = jnp.exp2((m_old - m_new) * CEXP)
            acc_ref[hm] = acc_ref[hm] * shrink + dot(values(hm // 2), weights)
            m_ref[hm] = m_new

    def tp_copy(src, dst, to, send, recv):
        return pltpu.make_async_remote_copy(
            src_ref=src, dst_ref=dst, send_sem=send, recv_sem=recv,
            device_id={"tp": to}, device_id_type=MESH,
        )

    def up(i):
        return lax.rem(tp + i, n_tp)

    def down(i):
        return lax.rem(tp + n_tp - i, n_tp)

    def x_copy(i):
        return tp_copy(xrows.at[tp], xrows.at[tp], up(i), x_send.at[i], x_recv.at[i])

    def stage_rows():
        take_slots(landed, d_send, d_recv)
        unpack_tiles(landed)
        for j in range(n_lane):
            xrows[tp, :, j * LANES : (j + 1) * LANES] = wide[pl.ds(j, slots, stride=n_lane), :].astype(BF16)
        for i in range(1, n_tp):
            x_copy(i).start()

    def p_copy(i):
        return tp_copy(part.at[down(i)], precv.at[tp], down(i), p_send.at[i], p_recv.at[i])

    def p_arrival(i):
        here = precv.at[up(i)]
        return tp_copy(here, here, up(i), p_send.at[i], p_recv.at[i])

    def stage_experts():
        for copy in weight_copies[:3]:
            copy.wait()

        def one(i, _):
            source = down(i)

            @pl.when(i > 0)
            def _():
                here = xrows.at[source]
                tp_copy(here, here, source, x_send.at[i], x_recv.at[i]).wait_recv()

            x_in = xrows[source]
            cols = min(fe, 256)
            for c0 in range(0, fe, cols):
                gate = jnp.minimum(dot(x_in, gw[:, c0 : c0 + cols]), CLAMP_LIMIT)
                lift = jnp.clip(dot(x_in, uw[:, c0 : c0 + cols]), -CLAMP_LIMIT, CLAMP_LIMIT)
                act[:, c0 : c0 + cols] = (gate * jax.nn.sigmoid(SIGMOID_SCALE * gate) * (lift + 1.0)).astype(BF16)
            for c0 in range(0, width, step_cols):
                part[source, :, c0 : c0 + step_cols] = dot(act[...], dw[:, c0 : c0 + step_cols]).astype(BF16)

            @pl.when(i > 0)
            def _():
                p_copy(i).start()

            return 0

        lax.fori_loop(0, n_tp, one, 0)

    def stage_return():
        flush_slots(packed, landed, d_send, d_recv)
        for i in range(1, n_tp):
            p_arrival(i).wait_recv()
        for j in range(n_lane):
            c = slice(j * LANES, (j + 1) * LANES)
            total = part[tp, :, c].astype(F32)
            for i in range(1, n_tp):
                total = total + precv[up(i), :, c].astype(F32)
            to_tiles(j, total)
        pack_tiles(packed)
        send_slots(packed, returned, e_send, e_recv)

    def step(t, _):
        s = t // 2 + 1
        u = lax.rem(t, 2)

        @pl.when(u == 0)
        def _():
            hop(K, R, s)
            hop(K, L, s)

        @pl.when(u == 1)
        def _():
            hop(V, R, s)
            hop(V, L, s)

        done = s - 1

        @pl.when(jnp.logical_and(u == 0, done < half))
        def _():
            across(K, R, done, 1 - core).wait_recv()
            across(V, R, done, 1 - core).wait_recv()

        @pl.when(jnp.logical_and(u == 1, done > 0))
        def _():
            across(K, L, done, 1 - core).wait_recv()
            across(V, L, done, 1 - core).wait_recv()

        @pl.when(t == 2 * half)
        def _():
            across(K, R, half, 1 - core).wait_recv()
            across(V, L, half, 1 - core).wait_recv()

        @pl.when(t != 1)
        def _():
            absorb_chip(lax.rem(z + n_z + jnp.where(u == 0, -done, done), n_z))

        @pl.when(t == stages[0])
        def _():
            stage_rows()

        @pl.when(t == stages[1])
        def _():
            stage_experts()

        @pl.when(t == stages[2])
        def _():
            stage_return()

        return 0

    lax.fori_loop(0, 2 * half + 1, step, 0)

    for h in range(heads):
        one = acc_ref[2 * h, 0:DV] / acc_ref[2 * h, DV : DV + 1]
        two = acc_ref[2 * h + 1, 0:DV] / acc_ref[2 * h + 1, DV : DV + 1]
        differ = one - lam_ref[h] * two
        scale = lax.rsqrt(jnp.mean(differ * differ, axis=0, keepdims=True) + HEAD_EPS)
        hr_ref[DV * h : DV * h + DV, :] = differ * scale * gain_ref[...] * OUT_SCALE
    weight_copies[3].wait()
    head_rows = hr_ref[...].T.astype(BF16)
    for c0 in range(0, width, step_cols):
        share = dot(head_rows, ow[:, c0 : c0 + step_cols]).astype(BF16)
        for d in range(n_tp):
            mp[d, :, c0 : c0 + step_cols] = share[tokens * d : tokens * (d + 1)]

    def m_copy(i):
        return tp_copy(mp.at[up(i)], mrecv.at[tp], up(i), m_send.at[i], m_recv.at[i])

    def m_arrival(i):
        here = mrecv.at[down(i)]
        return tp_copy(here, here, down(i), m_send.at[i], m_recv.at[i])

    for i in range(1, n_tp):
        m_copy(i).start()

    take_slots(returned, e_send, e_recv)
    unpack_tiles(returned)
    for j in range(n_lane):
        comb[:, j * LANES : (j + 1) * LANES] = wide[pl.ds(j, slots, stride=n_lane), :].astype(BF16)
    logits = logit_ref[...]
    low, high = logits[:, 0:1], logits[:, 1:2]
    combined = dot(picks(slot_first, slots), comb[...]) * (1.0 / (1.0 + jnp.exp(high - low)))
    combined = combined + dot(picks(slot_second, slots), comb[...]) * (1.0 / (jnp.exp(low - high) + 1.0))
    post = lax.rsqrt(jnp.mean(combined * combined, axis=-1, keepdims=True) + POST_EPS)
    eo_ref[...] = (combined * post).astype(BF16)

    for i in range(1, n_tp):
        m_arrival(i).wait_recv()
    mixed = mp[tp].astype(F32)
    for i in range(1, n_tp):
        mixed = mixed + mrecv[down(i)].astype(F32)
    mix_ref[...] = mixed.astype(BF16)

    flush_slots(packed, returned, e_send, e_recv)
    for i in range(1, n_tp):
        x_copy(i).wait_send()
        p_copy(i).wait_send()
        m_copy(i).wait_send()
    for a in (K, V):
        across(a, R, 0, core).wait_send()
        for direction in (R, L):

            def gone(s, _, a=a, direction=direction):
                ring_copy(a, direction, s).wait_send()
                across(a, direction, s, core).wait_send()
                return 0

            lax.fori_loop(1, limits[a][direction] + 1, gone, 0)


def local(
    n_ep, n_tp,
    queries, key_rows, value_rows, mix_lambda, head_gain, out_weight, expert_in, expert_gain,
    routes, route_logits, gate_weight, up_weight, down_weight,
):
    rows, cols = queries.shape
    heads = cols // (2 * DQK)
    tokens, width = expert_in.shape
    fe = gate_weight.shape[2]
    top = routes.shape[1]
    cap = (5 * tokens * top + 4 * n_ep - 1) // (4 * n_ep)
    slots = n_ep * cap
    n_lane = width // LANES
    half = n_ep // 4
    last = 2 * half
    stages = (min(2, last), min(6, last), min(11, last))
    dma = pltpu.SemaphoreType.DMA
    vmem = pl.BlockSpec(memory_space=pltpu.VMEM)
    whole = pl.BlockSpec(memory_space=pl.ANY)
    out = jax.ShapeDtypeStruct((tokens, width), BF16)
    return pl.pallas_call(
        functools.partial(kernel, n_ep, n_tp, cap, stages),
        out_shape=(out, out),
        in_specs=[vmem, vmem, vmem, pl.BlockSpec(memory_space=pltpu.SMEM), vmem, vmem, vmem, vmem, vmem]
        + [whole] * 4,
        out_specs=(vmem, vmem),
        scratch_shapes=[
            pltpu.VMEM((n_ep, rows, cols), BF16),
            pltpu.VMEM((n_ep, heads * DV, rows), BF16),
            pltpu.VMEM((2 * heads, GROUP, rows), BF16),
            pltpu.VMEM((2 * heads, 1, rows), F32),
            pltpu.VMEM((2 * heads, DV + ONES, rows), F32),
            pltpu.VMEM((width, fe), BF16),
            pltpu.VMEM((width, fe), BF16),
            pltpu.VMEM((fe, width), BF16),
            pltpu.VMEM(out_weight.shape, BF16),
            pltpu.VMEM((slots * n_lane, LANES), F32),
            pltpu.VMEM((slots, n_lane, LANES), BF16),
            pltpu.VMEM((slots, n_lane, LANES), BF16),
            pltpu.VMEM((n_tp, slots, width), BF16),
            pltpu.VMEM((slots, fe), BF16),
            pltpu.VMEM((n_tp, slots, width), BF16),
            pltpu.VMEM((n_tp, slots, width), BF16),
            pltpu.VMEM((slots, n_lane, LANES), BF16),
            pltpu.VMEM((slots, width), BF16),
            pltpu.VMEM((heads * DV, rows), F32),
            pltpu.VMEM((n_tp, tokens, width), BF16),
            pltpu.VMEM((n_tp, tokens, width), BF16),
            dma((4,)),
            dma((n_ep,)), dma((n_ep,)),
            dma((2, 2, half + 1)), dma((2, 2, half + 1)),
            dma((2, 2, half + 1)), dma((2, 2, half + 1)),
            dma((n_tp,)), dma((n_tp,)),
            dma((n_tp,)), dma((n_tp,)),
            dma((n_ep,)), dma((n_ep,)),
            dma((n_tp,)), dma((n_tp,)),
        ],
        compiler_params=pltpu.CompilerParams(
            collective_id=0, has_side_effects=True, vmem_limit_bytes=63 * 1024 * 1024
        ),
        name="mixer_and_experts",
    )(
        queries, key_rows, value_rows, mix_lambda, head_gain.reshape(DV, 1), expert_in,
        expert_gain.reshape(1, width), routes, route_logits, out_weight,
        gate_weight[0], up_weight[0], down_weight[0],
    )


def solution(mesh):
    every = ("grp", "ep", "tp")
    return jax.shard_map(
        functools.partial(local, mesh.shape["ep"], mesh.shape["tp"]),
        mesh=mesh,
        in_specs=(
            P(("grp", "ep"), "tp"), P(("grp", "ep"), "tp"), P(("grp", "ep"), "tp"),
            P("tp"), P(), P("tp", None), P(every, None), P(), P(every, None), P(every, None),
            P("ep", None, "tp"), P("ep", None, "tp"), P("ep", "tp", None),
        ),
        out_specs=(P(every, None), P(every, None)),
        check_vma=False,
    )
```

time: 501 us -> 209 us (0.42)
  Pallas kernels: 0 us -> 200 us
  blocking collectives: 134 us -> 0 us
  matrix products: 114 us -> 0 us
  other arithmetic: 89.7 us -> 0 us
  waiting for transfers between devices: 68.5 us -> 0 us
  local copies, waits for them, and re-layouts: 58.8 us -> 7.46 us
  starting transfers between devices: 19.4 us -> 0 us
  between operations: 14.4 us -> 0.64 us
    pallas_call x0 -> x1, Pallas kernels: none -> 200 us  [local(): pl.pallas_call(functools.partial(kernel, n_ep, n_tp, cap, stages), out_sh...]
    all_to_all x4 -> x0, blocking collectives: 134 us -> none  [the longest x2 68.7 us: exchange_in_order(): whole = lax.all_to_all(whole, axes[k], k, k, tiled=True)]
    dot_general x36 -> x0, matrix products: 114 us -> none  [the longest x16 72.7 us: step_block(): jnp.einsum('qhmd,khmd->hmqk', query_heads, key_block, preferred_element_t...]
    reduce_sum x25 -> x0, other arithmetic: 86.6 us -> none  [the longest x16 78.8 us: step_block(): running_sum = running_sum * shrink + jnp.sum(exponents, axis=-1)]
    all_to_all x2 -> x0, waiting for transfers between devices: 68.5 us -> none  [the longest x1 54.8 us: local(): lax.all_to_all(returned, EP, split_axis=0, concat_axis=0, tiled=True)]
    dynamic_slice x16 -> x0, local copies, waits for them, and re-layouts: 20.5 us -> none  [step_block(): lax.dynamic_slice_in_dim(value_piece, block_index * block_len, block_len, 0)]
    all_to_all x2 -> x0, starting transfers between devices: 19.3 us -> none  [the longest x1 15 us: local(): lax.all_to_all(returned, EP, split_axis=0, concat_axis=0, tiled=True)]
    while x48 -> x0, local copies, waits for them, and re-layouts: 12.7 us -> none
  transfers between devices with their start and end apart: 3 -> 0, of which waited for: 2 -> 0; matrix products, arithmetic and copies ran while one was open for 5% -> 0% of each run, Pallas kernels for 0% -> 0%
where the time goes in v1:
time: 209 us; the launch traced here: 208 us
  Pallas kernels  200 us (96%)
  local copies, waits for them, and re-layouts  7.46 us (4%)
    pallas_call x1, Pallas kernels, local(): pl.pallas_call(functools.partial(kernel, n_ep, n_tp, cap, stages), out_sh...  200 us
    unnamed x4, local copies, waits for them, and re-layouts  6.1 us

profile of v1, /device:TPU:33, one launch (start us, length us, event | category | flops | bytes accessed | tf_op | source)
XLA Modules:
  0.0 208.3 jit_solution(2156560341846239493)
XLA Ops:
  0.6 1.4 copy.15.gain_ref
  2.0 1.4 copy.16.routes_ref
  3.4 1.4 copy.17.logit_ref
  4.7 200.2 %mixer_and_experts.1 = (bf16[64,2048]{1,0:T(8,128)(2,1)}, bf16[64,2048]{1,0:T(8,128)(2,1)}) custom-call(bf16[256,512]{1,0:T(8,128)(2,1)} %q_ref.1, bf16[256,512]{1,0:T(8,128)(2,1)} %k_ref.1, bf16[256,512]{1,0:T(8,128)(2,1)} %v_ref.1, f32[8]{0:T(128)} %lam_ref.1, f32[64,1]{1,0:T(8,128)} %copy.15.gain_ref, bf16[64,2048]{1,0:T(8,128)(2,1)} %x_ref.1, ...), custom_call_target="tpu_custom_call" | custom-call | tf_op jit(solution)/shard_map/mixer_and_experts/pallas_call | solution.py:463
  205.0 1.7 copy.20
  206.7 1.7 copy.21

commit v2 on v1

--- a/solution.py
+++ b/solution.py
@@ -18,13 +18,11 @@
 OUT_SCALE = 0.8
 CEXP = DQK ** -0.5 * math.log2(math.e)
 LANES = 128
-GROUP = 256
+PAIR = 2 * DQK + DV
 ONES = 16
 LOOK = 2
 MESH = pl.DeviceIdType.MESH
 F32, BF16 = jnp.float32, jnp.bfloat16
-K, V = 0, 1
-R, L = 0, 1
 
 
 def dot(a, b):
@@ -36,20 +34,24 @@
     q_ref, k_ref, v_ref, lam_ref, gain_ref, x_ref, eg_ref, routes_ref, logit_ref,
     ow_hbm, gw_hbm, uw_hbm, dw_hbm,
     mix_ref, eo_ref,
-    kbuf, vbuf, q_mask, m_ref, acc_ref,
+    kv_out, kv_in, q_out, q_in, q_mask, vt_ref, m_ref, acc_ref, h_out, h_in,
     gw, uw, dw, ow,
-    wide, packed, landed, xrows, act, part, precv, returned, comb, hr_ref, mp, mrecv,
-    wsem, d_send, d_recv, r_send, r_recv, b_send, b_recv,
+    wide, packed, landed, xrows, act, part, precv, returned, comb, mp, mrecv,
+    wsem, d_send, d_recv, q_send, q_recv, k_send, k_recv, f_send, b_send, b_recv, h_send, h_recv,
     x_send, x_recv, p_send, p_recv, e_send, e_recv, m_send, m_recv,
 ):
     ep, tp = lax.axis_index("ep"), lax.axis_index("tp")
     n_z = n_ep // 2
-    half = n_z // 2
+    depth = n_z // 2
     z, core = ep // 2, lax.rem(ep, 2)
     sibling = 2 * z + 1 - core
+    head, odd = z // 2, lax.rem(z, 2)
+    partner = z + 1 - 2 * odd
+    parts = n_ep // 4
+    quarter = ep // parts
     rows = q_ref.shape[0]
     heads = q_ref.shape[1] // (2 * DQK)
-    maps = 2 * heads
+    units = 2 * parts
     tokens, width = x_ref.shape
     n_lane = width // LANES
     slots = n_ep * cap
@@ -76,39 +78,40 @@
     lax.fori_loop(1, n_tp, greet_tp, 0)
 
     routes = routes_ref[...].astype(F32)
-    first, second = routes[:, 0:1], routes[:, 1:2]
-    experts = lax.broadcasted_iota(jnp.int32, (tokens, n_ep), 1).astype(F32)
+    first, second = routes[0:1], routes[1:2]
+    experts = lax.broadcasted_iota(jnp.int32, (n_ep, tokens), 0).astype(F32)
     is_first = (first == experts).astype(F32)
     is_second = (second == experts).astype(F32)
     earlier = (
         lax.broadcasted_iota(jnp.int32, (tokens, tokens), 0)
-        > lax.broadcasted_iota(jnp.int32, (tokens, tokens), 1)
+        < lax.broadcasted_iota(jnp.int32, (tokens, tokens), 1)
     ).astype(BF16)
-    ahead = dot(earlier, (is_first + is_second).astype(BF16))
-    slot_first = first * cap + jnp.sum(ahead * is_first, axis=1, keepdims=True)
-    slot_second = second * cap + jnp.sum(ahead * is_second, axis=1, keepdims=True)
-
-    def picks(slot, count):
-        grid = lax.broadcasted_iota(jnp.int32, (tokens, count), 1).astype(F32)
+    ahead = dot((is_first + is_second).astype(BF16), earlier)
+    slot_first = first * cap + jnp.sum(ahead * is_first, axis=0, keepdims=True)
+    slot_second = second * cap + jnp.sum(ahead * is_second, axis=0, keepdims=True)
+
+    def picks(slot):
+        grid = lax.broadcasted_iota(jnp.int32, (slots, tokens), 0).astype(F32)
         return (slot == grid).astype(BF16)
+
+    def column(row):
+        n = row.shape[1]
+        eye = lax.broadcasted_iota(jnp.int32, (n, n), 0) == lax.broadcasted_iota(jnp.int32, (n, n), 1)
+        return jnp.sum(jnp.where(eye, row, 0.0), axis=1, keepdims=True)
 
     x = x_ref[...].astype(F32)
     normed = x * lax.rsqrt(jnp.mean(x * x, axis=-1, keepdims=True) + NORM_EPS)
     normed = (normed * eg_ref[...]).astype(BF16)
-    padded = -(-slots // LANES) * LANES
-    placing = (picks(slot_first, padded) + picks(slot_second, padded)).astype(BF16)
+    placing = picks(slot_first) + picks(slot_second)
 
     def to_tiles(j, columns):
         wide[pl.ds(j, slots, stride=n_lane), :] = columns
 
     step_cols = min(width, 512)
     for c0 in range(0, width, step_cols):
-        placed = lax.dot_general(
-            placing, normed[:, c0 : c0 + step_cols], (((0,), (0,)), ((), ())),
-            preferred_element_type=F32,
-        )
+        placed = dot(placing, normed[:, c0 : c0 + step_cols])
         for c1 in range(0, step_cols, LANES):
-            to_tiles((c0 + c1) // LANES, placed[:slots, c1 : c1 + LANES])
+            to_tiles((c0 + c1) // LANES, placed[:, c1 : c1 + LANES])
 
     def pack_tiles(dst):
         def one(i, _):
@@ -128,17 +131,14 @@
 
     pack_tiles(packed)
 
-    kbuf[ep] = k_ref[...]
-    vbuf[ep] = v_ref[...].astype(F32).T.astype(BF16)
-    q_cols = q_ref[...].astype(F32).T
-    row_map = lax.broadcasted_iota(jnp.int32, (GROUP, rows), 0) // DQK
-    per_group = GROUP // DQK
-    for hm in range(maps):
-        g = hm // per_group
-        block = q_cols[GROUP * g : GROUP * g + GROUP]
-        q_mask[hm] = jnp.where(row_map == hm % per_group, block, 0.0).astype(BF16)
-        m_ref[hm] = jnp.full((1, rows), -1e30, F32)
-        acc_ref[hm] = jnp.zeros((DV + ONES, rows), F32)
+    q_out[...] = q_ref[...].astype(F32).T.reshape(heads, 2 * DQK, rows).astype(BF16)
+    for h in range(heads):
+        c = slice(DV * h, DV * h + DV)
+        kv_out[h] = jnp.concatenate([k_ref[:, c].astype(F32), v_ref[:, c].astype(F32)], axis=1).astype(BF16)
+    vt_ref[DV:, :] = jnp.ones((ONES, 2 * rows), BF16)
+    for u in range(units):
+        m_ref[u] = jnp.full((1, rows), -1e30, F32)
+        acc_ref[u] = jnp.zeros((DV + ONES, rows), F32)
 
     pl.semaphore_wait(barrier, n_ep - 1 + n_tp - 1)
 
@@ -183,81 +183,119 @@
 
         lax.fori_loop(1, n_ep, one, 0)
 
-    send_slots(packed, landed, d_send, d_recv)
-
-    bufs = (kbuf, vbuf)
-    limits = ((half, half - 1), (half - 1, half))
-
-    def block_at(direction, s):
-        return lax.rem(z + n_z - s, n_z) if direction == R else lax.rem(z + s, n_z)
-
-    def ring_copy(a, direction, s):
-        there = bufs[a].at[2 * block_at(direction, s - 1) + core]
-        to = lax.rem(ep + 2, n_ep) if direction == R else lax.rem(ep + n_ep - 2, n_ep)
+    def remote(src, dst, send, recv, to):
         return pltpu.make_async_remote_copy(
-            src_ref=there, dst_ref=there,
-            send_sem=r_send.at[a, direction, s], recv_sem=r_recv.at[a, direction, s],
+            src_ref=src, dst_ref=dst, send_sem=send, recv_sem=recv,
             device_id={"ep": to}, device_id_type=MESH,
         )
 
-    def ring_arrival(a, direction, s):
-        here = bufs[a].at[2 * block_at(direction, s) + core]
-        source = lax.rem(ep + n_ep - 2, n_ep) if direction == R else lax.rem(ep + 2, n_ep)
-        return pltpu.make_async_remote_copy(
-            src_ref=here, dst_ref=here,
-            send_sem=r_send.at[a, direction, s], recv_sem=r_recv.at[a, direction, s],
-            device_id={"ep": source}, device_id_type=MESH,
-        )
-
-    def across(a, direction, s, owner):
-        here = bufs[a].at[2 * block_at(direction, s) + owner]
-        return pltpu.make_async_remote_copy(
-            src_ref=here, dst_ref=here,
-            send_sem=b_send.at[a, direction, s], recv_sem=b_recv.at[a, direction, s],
-            device_id={"ep": sibling}, device_id_type=MESH,
-        )
-
-    for a in (K, V):
-        for direction in (R, L):
-            ring_copy(a, direction, 1).start()
-        across(a, R, 0, core).start()
-
-    def hop(a, direction, s):
-        limit = limits[a][direction]
-
-        @pl.when(s <= limit)
-        def _():
-            ring_arrival(a, direction, s).wait_recv()
-
-            @pl.when(s < limit)
+    def each(count, act_on, body, own):
+        def one(i, _):
+            @pl.when(act_on(i) != ep)
             def _():
-                ring_copy(a, direction, s + 1).start()
-
-            across(a, direction, s, core).start()
+                body(i)
+
+            if own is not None:
+
+                @pl.when(act_on(i) == ep)
+                def _():
+                    own(i)
+
+            return 0
+
+        lax.fori_loop(0, count, one, 0)
+
+    def attends(h):
+        return 4 * h + quarter
+
+    def asks(i):
+        return parts * lax.rem(ep, 4) + i
+
+    def q_copy(h):
+        return remote(q_out.at[h], q_in.at[lax.rem(ep, parts)], q_send.at[h], q_recv.at[lax.rem(ep, parts)], attends(h))
+
+    def q_arrival(i):
+        return remote(q_in.at[i], q_in.at[i], q_send.at[0], q_recv.at[i], asks(i))
+
+    def q_own(h):
+        q_in[lax.rem(ep, parts)] = q_out[h]
+
+    each(heads, attends, lambda h: q_copy(h).start(), q_own)
+
+    def kv_copy(j):
+        pair = lax.rem(head + j, heads)
+        rightward = 2 * j - odd < depth
+        to = 2 * pair + jnp.where(rightward, 0, 1)
+        return remote(kv_out.at[pair], kv_in.at[ep], k_send.at[j], k_recv.at[z], 2 * to + core)
+
+    def side(k):
+        return lax.rem(z + n_z + jnp.where(odd == 1, k, -k), n_z)
+
+    def far_side(k):
+        return lax.rem(partner + n_z + jnp.where(odd == 1, -k, k), n_z)
+
+    def kv_arrival(chip):
+        here = kv_in.at[2 * chip + core]
+        return remote(here, here, k_send.at[0], k_recv.at[chip], 2 * partner + core)
+
+    def onward(chip):
+        here = kv_in.at[2 * chip + core]
+        return remote(here, here, f_send.at[chip], k_recv.at[chip], 2 * partner + core)
+
+    def across(chip, owner):
+        here = kv_in.at[2 * chip + owner]
+        return remote(here, here, b_send.at[chip], b_recv.at[chip], sibling)
+
+    kv_in[ep] = kv_out[head]
+    for j in (1, heads - 1):
+        if heads > 2 or j == 1:
+            kv_copy(j).start()
+        if heads == 2:
+            break
+    onward(z).start()
+    across(z, core).start()
+    send_slots(packed, landed, d_send, d_recv)
+
+    def kv_rest(j, _):
+        kv_copy(j).start()
+        kv_copy(heads - j).start()
+        return 0
+
+    if heads > 2:
+        lax.fori_loop(2, heads // 2, kv_rest, 0)
+        kv_copy(heads // 2).start()
+
+    each(parts, asks, lambda i: q_arrival(i).wait_recv(), None)
+    row_map = lax.broadcasted_iota(jnp.int32, (PAIR, rows), 0) // DQK
+
+    def mask_queries(i, _):
+        block = jnp.concatenate([q_in[i].astype(F32), jnp.zeros((DV, rows), F32)], axis=0)
+        for m in (0, 1):
+            q_mask[2 * i + m] = jnp.where(row_map == m, block, 0.0).astype(BF16)
+        return 0
+
+    lax.fori_loop(0, parts, mask_queries, 0)
 
     def absorb_chip(chip):
-        ones = jnp.ones((ONES, 2 * rows), BF16)
-
-        def score(hm):
-            c0 = GROUP * (hm // per_group)
-            keys = jnp.concatenate([kbuf[2 * chip + b, :, c0 : c0 + GROUP] for b in (0, 1)], axis=0)
-            return dot(keys, q_mask[hm])
-
-        def values(h):
-            cols = [vbuf[2 * chip + b, DV * h : DV * h + DV, :] for b in (0, 1)]
-            return jnp.concatenate([jnp.concatenate(cols, axis=1), ones], axis=0)
-
-        pending = [score(i) for i in range(min(LOOK, maps))]
-        for hm in range(maps):
-            if hm + LOOK < maps:
-                pending.append(score(hm + LOOK))
+        for b in (0, 1):
+            turned = kv_in[2 * chip + b].astype(F32).T
+            vt_ref[0:DV, b * rows : (b + 1) * rows] = turned[2 * DQK :].astype(BF16)
+
+        def score(u):
+            keys = jnp.concatenate([kv_in[2 * chip + b] for b in (0, 1)], axis=0)
+            return dot(keys, q_mask[u])
+
+        pending = [score(i) for i in range(min(LOOK, units))]
+        for u in range(units):
+            if u + LOOK < units:
+                pending.append(score(u + LOOK))
             s = pending.pop(0)
-            m_old = m_ref[hm]
+            m_old = m_ref[u]
             m_new = jnp.maximum(m_old, jnp.max(s, axis=0, keepdims=True))
             weights = jnp.exp2(s * CEXP - m_new * CEXP).astype(BF16)
             shrink = jnp.exp2((m_old - m_new) * CEXP)
-            acc_ref[hm] = acc_ref[hm] * shrink + dot(values(hm // 2), weights)
-            m_ref[hm] = m_new
+            acc_ref[u] = acc_ref[u] * shrink + dot(vt_ref[...], weights)
+            m_ref[u] = m_new
 
     def tp_copy(src, dst, to, send, recv):
         return pltpu.make_async_remote_copy(
@@ -332,39 +370,25 @@
         send_slots(packed, returned, e_send, e_recv)
 
     def step(t, _):
-        s = t // 2 + 1
-        u = lax.rem(t, 2)
-
-        @pl.when(u == 0)
+        k = t // 2
+        near = lax.rem(t, 2) == 0
+
+        @pl.when(jnp.logical_and(near, k + 1 < depth))
         def _():
-            hop(K, R, s)
-            hop(K, L, s)
-
-        @pl.when(u == 1)
+            chip = side(k + 1)
+            kv_arrival(chip).wait_recv()
+            onward(chip).start()
+            across(chip, core).start()
+
+        @pl.when(near)
         def _():
-            hop(V, R, s)
-            hop(V, L, s)
-
-        done = s - 1
-
-        @pl.when(jnp.logical_and(u == 0, done < half))
-        def _():
-            across(K, R, done, 1 - core).wait_recv()
-            across(V, R, done, 1 - core).wait_recv()
-
-        @pl.when(jnp.logical_and(u == 1, done > 0))
-        def _():
-            across(K, L, done, 1 - core).wait_recv()
-            across(V, L, done, 1 - core).wait_recv()
-
-        @pl.when(t == 2 * half)
-        def _():
-            across(K, R, half, 1 - core).wait_recv()
-            across(V, L, half, 1 - core).wait_recv()
-
-        @pl.when(t != 1)
-        def _():
-            absorb_chip(lax.rem(z + n_z + jnp.where(u == 0, -done, done), n_z))
+            chip = far_side(k)
+            kv_arrival(chip).wait_recv()
+            across(chip, core).start()
+
+        chip = jnp.where(near, side(k), far_side(k))
+        across(chip, 1 - core).wait_recv()
+        absorb_chip(chip)
 
         @pl.when(t == stages[0])
         def _():
@@ -380,16 +404,35 @@
 
         return 0
 
-    lax.fori_loop(0, 2 * half + 1, step, 0)
-
-    for h in range(heads):
-        one = acc_ref[2 * h, 0:DV] / acc_ref[2 * h, DV : DV + 1]
-        two = acc_ref[2 * h + 1, 0:DV] / acc_ref[2 * h + 1, DV : DV + 1]
-        differ = one - lam_ref[h] * two
+    lax.fori_loop(0, 2 * depth, step, 0)
+
+    lam = lam_ref[head]
+    gain = column(gain_ref[...]) * OUT_SCALE
+
+    def finish(i, _):
+        one = acc_ref[2 * i, 0:DV] / acc_ref[2 * i, DV : DV + 1]
+        two = acc_ref[2 * i + 1, 0:DV] / acc_ref[2 * i + 1, DV : DV + 1]
+        differ = one - lam * two
         scale = lax.rsqrt(jnp.mean(differ * differ, axis=0, keepdims=True) + HEAD_EPS)
-        hr_ref[DV * h : DV * h + DV, :] = differ * scale * gain_ref[...] * OUT_SCALE
+        h_out[i] = (differ * scale * gain).astype(BF16)
+        return 0
+
+    lax.fori_loop(0, parts, finish, 0)
+
+    def h_copy(i):
+        return remote(h_out.at[i], h_in.at[head], h_send.at[i], h_recv.at[head], asks(i))
+
+    def h_arrival(h):
+        return remote(h_in.at[h], h_in.at[h], h_send.at[0], h_recv.at[h], attends(h))
+
+    def h_own(i):
+        h_in[head] = h_out[i]
+
+    each(parts, asks, lambda i: h_copy(i).start(), h_own)
     weight_copies[3].wait()
-    head_rows = hr_ref[...].T.astype(BF16)
+    each(heads, attends, lambda h: h_arrival(h).wait_recv(), None)
+
+    head_rows = h_in[...].astype(F32).reshape(heads * DV, rows).T.astype(BF16)
     for c0 in range(0, width, step_cols):
         share = dot(head_rows, ow[:, c0 : c0 + step_cols]).astype(BF16)
         for d in range(n_tp):
@@ -410,9 +453,13 @@
     for j in range(n_lane):
         comb[:, j * LANES : (j + 1) * LANES] = wide[pl.ds(j, slots, stride=n_lane), :].astype(BF16)
     logits = logit_ref[...]
-    low, high = logits[:, 0:1], logits[:, 1:2]
-    combined = dot(picks(slot_first, slots), comb[...]) * (1.0 / (1.0 + jnp.exp(high - low)))
-    combined = combined + dot(picks(slot_second, slots), comb[...]) * (1.0 / (jnp.exp(low - high) + 1.0))
+    low, high = logits[0:1], logits[1:2]
+
+    def picked(slot):
+        return lax.dot_general(picks(slot), comb[...], (((0,), (0,)), ((), ())), preferred_element_type=F32)
+
+    combined = picked(slot_first) * column(1.0 / (1.0 + jnp.exp(high - low)))
+    combined = combined + picked(slot_second) * column(1.0 / (jnp.exp(low - high) + 1.0))
     post = lax.rsqrt(jnp.mean(combined * combined, axis=-1, keepdims=True) + POST_EPS)
     eo_ref[...] = (combined * post).astype(BF16)
 
@@ -428,16 +475,22 @@
         x_copy(i).wait_send()
         p_copy(i).wait_send()
         m_copy(i).wait_send()
-    for a in (K, V):
-        across(a, R, 0, core).wait_send()
-        for direction in (R, L):
-
-            def gone(s, _, a=a, direction=direction):
-                ring_copy(a, direction, s).wait_send()
-                across(a, direction, s, core).wait_send()
-                return 0
-
-            lax.fori_loop(1, limits[a][direction] + 1, gone, 0)
+    each(heads, attends, lambda h: q_copy(h).wait_send(), None)
+    each(parts, asks, lambda i: h_copy(i).wait_send(), None)
+
+    def gone(j, _):
+        kv_copy(j).wait_send()
+        return 0
+
+    lax.fori_loop(1, heads, gone, 0)
+
+    def forwarded(k, _):
+        onward(side(k)).wait_send()
+        across(side(k), core).wait_send()
+        across(far_side(k), core).wait_send()
+        return 0
+
+    lax.fori_loop(0, depth, forwarded, 0)
 
 
 def local(
@@ -453,9 +506,10 @@
     cap = (5 * tokens * top + 4 * n_ep - 1) // (4 * n_ep)
     slots = n_ep * cap
     n_lane = width // LANES
-    half = n_ep // 4
-    last = 2 * half
-    stages = (min(2, last), min(6, last), min(11, last))
+    parts = n_ep // 4
+    last = n_ep // 2 - 1
+    stages = (min(5, last), min(9, last), min(13, last))
+    assert n_ep == 4 * heads
     dma = pltpu.SemaphoreType.DMA
     vmem = pl.BlockSpec(memory_space=pltpu.VMEM)
     whole = pl.BlockSpec(memory_space=pl.ANY)
@@ -467,11 +521,16 @@
         + [whole] * 4,
         out_specs=(vmem, vmem),
         scratch_shapes=[
-            pltpu.VMEM((n_ep, rows, cols), BF16),
-            pltpu.VMEM((n_ep, heads * DV, rows), BF16),
-            pltpu.VMEM((2 * heads, GROUP, rows), BF16),
-            pltpu.VMEM((2 * heads, 1, rows), F32),
-            pltpu.VMEM((2 * heads, DV + ONES, rows), F32),
+            pltpu.VMEM((heads, rows, PAIR), BF16),
+            pltpu.VMEM((n_ep, rows, PAIR), BF16),
+            pltpu.VMEM((heads, 2 * DQK, rows), BF16),
+            pltpu.VMEM((parts, 2 * DQK, rows), BF16),
+            pltpu.VMEM((2 * parts, PAIR, rows), BF16),
+            pltpu.VMEM((DV + ONES, 2 * rows), BF16),
+            pltpu.VMEM((2 * parts, 1, rows), F32),
+            pltpu.VMEM((2 * parts, DV + ONES, rows), F32),
+            pltpu.VMEM((parts, DV, rows), BF16),
+            pltpu.VMEM((heads, DV, rows), BF16),
             pltpu.VMEM((width, fe), BF16),
             pltpu.VMEM((width, fe), BF16),
             pltpu.VMEM((fe, width), BF16),
@@ -485,13 +544,13 @@
             pltpu.VMEM((n_tp, slots, width), BF16),
             pltpu.VMEM((slots, n_lane, LANES), BF16),
             pltpu.VMEM((slots, width), BF16),
-            pltpu.VMEM((heads * DV, rows), F32),
             pltpu.VMEM((n_tp, tokens, width), BF16),
             pltpu.VMEM((n_tp, tokens, width), BF16),
             dma((4,)),
             dma((n_ep,)), dma((n_ep,)),
-            dma((2, 2, half + 1)), dma((2, 2, half + 1)),
-            dma((2, 2, half + 1)), dma((2, 2, half + 1)),
+            dma((heads,)), dma((parts,)),
+            dma((heads,)), dma((n_ep // 2,)), dma((n_ep // 2,)), dma((n_ep // 2,)), dma((n_ep // 2,)),
+            dma((parts,)), dma((heads,)),
             dma((n_tp,)), dma((n_tp,)),
             dma((n_tp,)), dma((n_tp,)),
             dma((n_ep,)), dma((n_ep,)),
@@ -502,8 +561,8 @@
         ),
         name="mixer_and_experts",
     )(
-        queries, key_rows, value_rows, mix_lambda, head_gain.reshape(DV, 1), expert_in,
-        expert_gain.reshape(1, width), routes, route_logits, out_weight,
+        queries, key_rows, value_rows, mix_lambda, head_gain.reshape(1, DV), expert_in,
+        expert_gain.reshape(1, width), routes.T, route_logits.T, out_weight,
         gate_weight[0], up_weight[0], down_weight[0],
     )
 

time: 209 us -> 223 us (1.067)
  Pallas kernels: 200 us -> 219 us
  local copies, waits for them, and re-layouts: 7.46 us -> 3.34 us
    pallas_call x1, Pallas kernels: 200 us -> 219 us  [local(): pl.pallas_call(functools.partial(kernel, n_ep, n_tp, cap, stages), out_sh...]
    unnamed x4 -> x2, local copies, waits for them, and re-layouts: 6.1 us -> 3.34 us
where the time goes in v2:
time: 223 us
  Pallas kernels  219 us (98%)
  local copies, waits for them, and re-layouts  3.34 us (1%)
    pallas_call x1, Pallas kernels, local(): pl.pallas_call(functools.partial(kernel, n_ep, n_tp, cap, stages), out_sh...  219 us

profile of v2, /device:TPU:33, one launch (start us, length us, event | category | flops | bytes accessed | tf_op | source)
XLA Modules:
  0.0 222.6 jit_solution(7087856451832215219)
XLA Ops:
  0.6 218.6 %mixer_and_experts.1 = (bf16[64,2048]{1,0:T(8,128)(2,1)}, bf16[64,2048]{1,0:T(8,128)(2,1)}) custom-call(bf16[256,512]{1,0:T(8,128)(2,1)} %q_ref.1, bf16[256,512]{1,0:T(8,128)(2,1)} %k_ref.1, bf16[256,512]{1,0:T(8,128)(2,1)} %v_ref.1, f32[8]{0:T(128)} %lam_ref.1, f32[1,64]{1,0:T(1,128)} %bitcast.13, bf16[64,2048]{1,0:T(8,128)(2,1)} %x_ref.1, ...), custom_call_target="tpu_custom_call" | custom-call | tf_op jit(solution)/shard_map/mixer_and_experts/pallas_call | solution.py:517
  219.3 1.7 copy.17
  220.9 1.7 copy.18

commit v3 on v2

--- a/solution.py
+++ b/solution.py
@@ -20,7 +20,8 @@
 LANES = 128
 PAIR = 2 * DQK + DV
 ONES = 16
-LOOK = 2
+STAGES = (1, 5, 6, 10)
+LOOK = 3
 MESH = pl.DeviceIdType.MESH
 F32, BF16 = jnp.float32, jnp.bfloat16
 
@@ -36,7 +37,7 @@
     mix_ref, eo_ref,
     kv_out, kv_in, q_out, q_in, q_mask, vt_ref, m_ref, acc_ref, h_out, h_in,
     gw, uw, dw, ow,
-    wide, packed, landed, xrows, act, part, precv, returned, comb, mp, mrecv,
+    wide, packed, landed, xrows, act, part, precv, going, returned, comb, mp, mrecv,
     wsem, d_send, d_recv, q_send, q_recv, k_send, k_recv, f_send, b_send, b_recv, h_send, h_recv,
     x_send, x_recv, p_send, p_recv, e_send, e_recv, m_send, m_recv,
 ):
@@ -56,6 +57,7 @@
     n_lane = width // LANES
     slots = n_ep * cap
     fe = gw.shape[1]
+    band = slots // 2
 
     weight_copies = [
         pltpu.make_async_copy(src, dst, wsem.at[i])
@@ -105,7 +107,7 @@
     placing = picks(slot_first) + picks(slot_second)
 
     def to_tiles(j, columns):
-        wide[pl.ds(j, slots, stride=n_lane), :] = columns
+        wide[pl.ds(j, columns.shape[0], stride=n_lane), :] = columns
 
     step_cols = min(width, 512)
     for c0 in range(0, width, step_cols):
@@ -113,23 +115,23 @@
         for c1 in range(0, step_cols, LANES):
             to_tiles((c0 + c1) // LANES, placed[:, c1 : c1 + LANES])
 
-    def pack_tiles(dst):
+    def pack_tiles(dst, base, count):
         def one(i, _):
             block = wide[pl.ds(pl.multiple_of(i * cap * n_lane, n_lane), cap * n_lane), :]
-            dst[pl.ds(i * cap, cap)] = block.reshape(cap, n_lane, LANES).astype(BF16)
+            dst[pl.ds(base + i * cap, cap)] = block.reshape(cap, n_lane, LANES).astype(BF16)
             return 0
 
-        lax.fori_loop(0, n_ep, one, 0)
-
-    def unpack_tiles(src):
+        lax.fori_loop(0, count, one, 0)
+
+    def unpack_tiles(src, base, count):
         def one(i, _):
-            block = src[pl.ds(i * cap, cap)].astype(F32)
+            block = src[pl.ds(base + i * cap, cap)].astype(F32)
             wide[pl.ds(pl.multiple_of(i * cap * n_lane, n_lane), cap * n_lane), :] = block.reshape(cap * n_lane, LANES)
             return 0
 
-        lax.fori_loop(0, n_ep, one, 0)
-
-    pack_tiles(packed)
+        lax.fori_loop(0, count, one, 0)
+
+    pack_tiles(packed, 0, n_ep)
 
     q_out[...] = q_ref[...].astype(F32).T.reshape(heads, 2 * DQK, rows).astype(BF16)
     for h in range(heads):
@@ -142,46 +144,54 @@
 
     pl.semaphore_wait(barrier, n_ep - 1 + n_tp - 1)
 
-    def slot_copy(src, dst, send, recv, d):
-        to = lax.rem(ep + d, n_ep)
+    fourth = n_ep // 4
+
+    def place(d):
+        return jnp.where(d <= fourth, d, jnp.where(d > 3 * fourth, d - 2 * fourth, d + fourth - 1))
+
+    def ep_copy(src, dst, send, recv, to):
         return pltpu.make_async_remote_copy(
-            src_ref=src.at[pl.ds(to * cap, cap)],
-            dst_ref=dst.at[pl.ds(ep * cap, cap)],
-            send_sem=send.at[d], recv_sem=recv.at[d],
+            src_ref=src, dst_ref=dst, send_sem=send, recv_sem=recv,
             device_id={"ep": to}, device_id_type=MESH,
         )
 
-    def slot_arrival(dst, send, recv, d):
-        source = lax.rem(ep + n_ep - d, n_ep)
-        here = dst.at[pl.ds(source * cap, cap)]
-        return pltpu.make_async_remote_copy(
-            src_ref=here, dst_ref=here, send_sem=send.at[d], recv_sem=recv.at[d],
-            device_id={"ep": source}, device_id_type=MESH,
-        )
-
-    def send_slots(src, dst, send, recv):
+    def ahead_of(d):
+        return lax.rem(ep + d, n_ep)
+
+    def behind(d):
+        return lax.rem(ep + n_ep - d, n_ep)
+
+    def out_copy(d):
+        to = ahead_of(d)
+        return ep_copy(packed.at[pl.ds(to * cap, cap)], landed.at[pl.ds(place(d) * cap, cap)], d_send.at[d], d_recv.at[d], to)
+
+    def out_arrival(d):
+        here = landed.at[pl.ds(place(d) * cap, cap)]
+        return ep_copy(here, here, d_send.at[d], d_recv.at[d], behind(d))
+
+    def back_copy(d):
+        return ep_copy(going.at[pl.ds(place(d) * cap, cap)], returned.at[pl.ds(ep * cap, cap)], e_send.at[d], e_recv.at[d], behind(d))
+
+    def back_arrival(d):
+        here = returned.at[pl.ds(ahead_of(d) * cap, cap)]
+        return ep_copy(here, here, e_send.at[d], e_recv.at[d], ahead_of(d))
+
+    def over_half(half, act_on):
         def pair(i, _):
-            slot_copy(src, dst, send, recv, i).start()
-            slot_copy(src, dst, send, recv, n_ep - i).start()
+            act_on(i)
+            act_on(n_ep - i)
             return 0
 
-        lax.fori_loop(1, n_ep // 2, pair, 0)
-        slot_copy(src, dst, send, recv, n_ep // 2).start()
-        dst[pl.ds(ep * cap, cap)] = src[pl.ds(ep * cap, cap)]
-
-    def take_slots(dst, send, recv):
-        def one(d, _):
-            slot_arrival(dst, send, recv, d).wait_recv()
-            return 0
-
-        lax.fori_loop(1, n_ep, one, 0)
-
-    def flush_slots(src, dst, send, recv):
-        def one(d, _):
-            slot_copy(src, dst, send, recv, d).wait_send()
-            return 0
-
-        lax.fori_loop(1, n_ep, one, 0)
+        if half == 0:
+            lax.fori_loop(1, fourth, pair, 0)
+            act_on(fourth)
+        else:
+            act_on(3 * fourth)
+            lax.fori_loop(fourth + 1, 2 * fourth, pair, 0)
+            act_on(2 * fourth)
+
+    over_half(0, lambda d: out_copy(d).start())
+    landed[0:cap] = packed[pl.ds(ep * cap, cap)]
 
     def remote(src, dst, send, recv, to):
         return pltpu.make_async_remote_copy(
@@ -246,32 +256,97 @@
         here = kv_in.at[2 * chip + owner]
         return remote(here, here, b_send.at[chip], b_recv.at[chip], sibling)
 
+    def kv_band(first, last):
+        def both(j, _):
+            kv_copy(j).start()
+            kv_copy(heads - j).start()
+            return 0
+
+        stop = heads // 2
+        lax.fori_loop(min(first, stop), min(last, stop), both, 0)
+        if first <= stop < last:
+            kv_copy(stop).start()
+
     kv_in[ep] = kv_out[head]
-    for j in (1, heads - 1):
-        if heads > 2 or j == 1:
-            kv_copy(j).start()
-        if heads == 2:
-            break
     onward(z).start()
     across(z, core).start()
-    send_slots(packed, landed, d_send, d_recv)
-
-    def kv_rest(j, _):
-        kv_copy(j).start()
-        kv_copy(heads - j).start()
-        return 0
-
-    if heads > 2:
-        lax.fori_loop(2, heads // 2, kv_rest, 0)
-        kv_copy(heads // 2).start()
+    kv_band(1, 3)
+    over_half(1, lambda d: out_copy(d).start())
+    kv_band(3, heads)
+
+    def tp_copy(src, dst, to, send, recv):
+        return pltpu.make_async_remote_copy(
+            src_ref=src, dst_ref=dst, send_sem=send, recv_sem=recv,
+            device_id={"tp": to}, device_id_type=MESH,
+        )
+
+    def up(i):
+        return lax.rem(tp + i, n_tp)
+
+    def down(i):
+        return lax.rem(tp + n_tp - i, n_tp)
+
+    def x_copy(half, i):
+        block = xrows.at[half, tp]
+        return tp_copy(block, block, up(i), x_send.at[half, i], x_recv.at[half, i])
+
+    def stage_rows(half):
+        over_half(half, lambda d: out_arrival(d).wait_recv())
+        unpack_tiles(landed, half * band, n_ep // 2)
+        for j in range(n_lane):
+            xrows[half, tp, :, j * LANES : (j + 1) * LANES] = wide[pl.ds(j, band, stride=n_lane), :].astype(BF16)
+        for i in range(1, n_tp):
+            x_copy(half, i).start()
+
+    def p_copy(half, i):
+        return tp_copy(part.at[half, down(i)], precv.at[half, tp], down(i), p_send.at[half, i], p_recv.at[half, i])
+
+    def stage_experts(half):
+        if half == 0:
+            for copy in weight_copies[:3]:
+                copy.wait()
+        for i in range(1, n_tp):
+            here = xrows.at[half, down(i)]
+            tp_copy(here, here, down(i), x_send.at[half, i], x_recv.at[half, i]).wait_recv()
+        x_in = xrows[half].reshape(n_tp * band, width)
+        cols = min(fe, 256)
+        for c0 in range(0, fe, cols):
+            gate = jnp.minimum(dot(x_in, gw[:, c0 : c0 + cols]), CLAMP_LIMIT)
+            lift = jnp.clip(dot(x_in, uw[:, c0 : c0 + cols]), -CLAMP_LIMIT, CLAMP_LIMIT)
+            act[:, c0 : c0 + cols] = (gate * jax.nn.sigmoid(SIGMOID_SCALE * gate) * (lift + 1.0)).astype(BF16)
+        for c0 in range(0, width, cols):
+            share = dot(act[...], dw[:, c0 : c0 + cols]).astype(BF16)
+            part[half, :, :, c0 : c0 + cols] = share.reshape(n_tp, band, cols)
+        for i in range(1, n_tp):
+            p_copy(half, i).start()
+
+    def stage_return(half):
+        for i in range(1, n_tp):
+            here = precv.at[half, up(i)]
+            tp_copy(here, here, up(i), p_send.at[half, i], p_recv.at[half, i]).wait_recv()
+        for j in range(n_lane):
+            c = slice(j * LANES, (j + 1) * LANES)
+            total = part[half, tp, :, c].astype(F32)
+            for i in range(1, n_tp):
+                total = total + precv[half, up(i), :, c].astype(F32)
+            to_tiles(j, total)
+        pack_tiles(going, half * band, n_ep // 2)
+        over_half(half, lambda d: back_copy(d).start())
+        if half == 0:
+            returned[pl.ds(ep * cap, cap)] = going[0:cap]
+
+    stage_rows(0)
 
     each(parts, asks, lambda i: q_arrival(i).wait_recv(), None)
     row_map = lax.broadcasted_iota(jnp.int32, (PAIR, rows), 0) // DQK
 
     def mask_queries(i, _):
-        block = jnp.concatenate([q_in[i].astype(F32), jnp.zeros((DV, rows), F32)], axis=0)
+        block = jnp.concatenate([q_in[i].astype(F32) * CEXP, jnp.zeros((DV, rows), F32)], axis=0)
         for m in (0, 1):
-            q_mask[2 * i + m] = jnp.where(row_map == m, block, 0.0).astype(BF16)
+            kept = jnp.where(row_map == m, block, 0.0)
+            high = kept.astype(BF16)
+            q_mask[2 * i + m, 0:PAIR] = high
+            q_mask[2 * i + m, PAIR:] = (kept - high.astype(F32)).astype(BF16)
         return 0
 
     lax.fori_loop(0, parts, mask_queries, 0)
@@ -283,7 +358,7 @@
 
         def score(u):
             keys = jnp.concatenate([kv_in[2 * chip + b] for b in (0, 1)], axis=0)
-            return dot(keys, q_mask[u])
+            return dot(jnp.concatenate([keys, keys], axis=1), q_mask[u])
 
         pending = [score(i) for i in range(min(LOOK, units))]
         for u in range(units):
@@ -292,82 +367,10 @@
             s = pending.pop(0)
             m_old = m_ref[u]
             m_new = jnp.maximum(m_old, jnp.max(s, axis=0, keepdims=True))
-            weights = jnp.exp2(s * CEXP - m_new * CEXP).astype(BF16)
-            shrink = jnp.exp2((m_old - m_new) * CEXP)
+            weights = jnp.exp2(s - m_new).astype(BF16)
+            shrink = jnp.exp2(m_old - m_new)
             acc_ref[u] = acc_ref[u] * shrink + dot(vt_ref[...], weights)
             m_ref[u] = m_new
-
-    def tp_copy(src, dst, to, send, recv):
-        return pltpu.make_async_remote_copy(
-            src_ref=src, dst_ref=dst, send_sem=send, recv_sem=recv,
-            device_id={"tp": to}, device_id_type=MESH,
-        )
-
-    def up(i):
-        return lax.rem(tp + i, n_tp)
-
-    def down(i):
-        return lax.rem(tp + n_tp - i, n_tp)
-
-    def x_copy(i):
-        return tp_copy(xrows.at[tp], xrows.at[tp], up(i), x_send.at[i], x_recv.at[i])
-
-    def stage_rows():
-        take_slots(landed, d_send, d_recv)
-        unpack_tiles(landed)
-        for j in range(n_lane):
-            xrows[tp, :, j * LANES : (j + 1) * LANES] = wide[pl.ds(j, slots, stride=n_lane), :].astype(BF16)
-        for i in range(1, n_tp):
-            x_copy(i).start()
-
-    def p_copy(i):
-        return tp_copy(part.at[down(i)], precv.at[tp], down(i), p_send.at[i], p_recv.at[i])
-
-    def p_arrival(i):
-        here = precv.at[up(i)]
-        return tp_copy(here, here, up(i), p_send.at[i], p_recv.at[i])
-
-    def stage_experts():
-        for copy in weight_copies[:3]:
-            copy.wait()
-
-        def one(i, _):
-            source = down(i)
-
-            @pl.when(i > 0)
-            def _():
-                here = xrows.at[source]
-                tp_copy(here, here, source, x_send.at[i], x_recv.at[i]).wait_recv()
-
-            x_in = xrows[source]
-            cols = min(fe, 256)
-            for c0 in range(0, fe, cols):
-                gate = jnp.minimum(dot(x_in, gw[:, c0 : c0 + cols]), CLAMP_LIMIT)
-                lift = jnp.clip(dot(x_in, uw[:, c0 : c0 + cols]), -CLAMP_LIMIT, CLAMP_LIMIT)
-                act[:, c0 : c0 + cols] = (gate * jax.nn.sigmoid(SIGMOID_SCALE * gate) * (lift + 1.0)).astype(BF16)
-            for c0 in range(0, width, step_cols):
-                part[source, :, c0 : c0 + step_cols] = dot(act[...], dw[:, c0 : c0 + step_cols]).astype(BF16)
-
-            @pl.when(i > 0)
-            def _():
-                p_copy(i).start()
-
-            return 0
-
-        lax.fori_loop(0, n_tp, one, 0)
-
-    def stage_return():
-        flush_slots(packed, landed, d_send, d_recv)
-        for i in range(1, n_tp):
-            p_arrival(i).wait_recv()
-        for j in range(n_lane):
-            c = slice(j * LANES, (j + 1) * LANES)
-            total = part[tp, :, c].astype(F32)
-            for i in range(1, n_tp):
-                total = total + precv[up(i), :, c].astype(F32)
-            to_tiles(j, total)
-        pack_tiles(packed)
-        send_slots(packed, returned, e_send, e_recv)
 
     def step(t, _):
         k = t // 2
@@ -392,15 +395,19 @@
 
         @pl.when(t == stages[0])
         def _():
-            stage_rows()
+            stage_experts(0)
 
         @pl.when(t == stages[1])
         def _():
-            stage_experts()
+            stage_return(0)
 
         @pl.when(t == stages[2])
         def _():
-            stage_return()
+            stage_rows(1)
+
+        @pl.when(t == stages[3])
+        def _():
+            stage_experts(1)
 
         return 0
 
@@ -429,6 +436,7 @@
         h_in[head] = h_out[i]
 
     each(parts, asks, lambda i: h_copy(i).start(), h_own)
+    stage_return(1)
     weight_copies[3].wait()
     each(heads, attends, lambda h: h_arrival(h).wait_recv(), None)
 
@@ -448,8 +456,9 @@
     for i in range(1, n_tp):
         m_copy(i).start()
 
-    take_slots(returned, e_send, e_recv)
-    unpack_tiles(returned)
+    for half in (0, 1):
+        over_half(half, lambda d: back_arrival(d).wait_recv())
+    unpack_tiles(returned, 0, n_ep)
     for j in range(n_lane):
         comb[:, j * LANES : (j + 1) * LANES] = wide[pl.ds(j, slots, stride=n_lane), :].astype(BF16)
     logits = logit_ref[...]
@@ -470,10 +479,13 @@
         mixed = mixed + mrecv[down(i)].astype(F32)
     mix_ref[...] = mixed.astype(BF16)
 
-    flush_slots(packed, returned, e_send, e_recv)
+    for half in (0, 1):
+        over_half(half, lambda d: out_copy(d).wait_send())
+        over_half(half, lambda d: back_copy(d).wait_send())
+        for i in range(1, n_tp):
+            x_copy(half, i).wait_send()
+            p_copy(half, i).wait_send()
     for i in range(1, n_tp):
-        x_copy(i).wait_send()
-        p_copy(i).wait_send()
         m_copy(i).wait_send()
     each(heads, attends, lambda h: q_copy(h).wait_send(), None)
     each(parts, asks, lambda i: h_copy(i).wait_send(), None)
@@ -508,7 +520,7 @@
     n_lane = width // LANES
     parts = n_ep // 4
     last = n_ep // 2 - 1
-    stages = (min(5, last), min(9, last), min(13, last))
+    stages = tuple(min(t, last) for t in STAGES)
     assert n_ep == 4 * heads
     dma = pltpu.SemaphoreType.DMA
     vmem = pl.BlockSpec(memory_space=pltpu.VMEM)
@@ -525,7 +537,7 @@
             pltpu.VMEM((n_ep, rows, PAIR), BF16),
             pltpu.VMEM((heads, 2 * DQK, rows), BF16),
             pltpu.VMEM((parts, 2 * DQK, rows), BF16),
-            pltpu.VMEM((2 * parts, PAIR, rows), BF16),
+            pltpu.VMEM((2 * parts, 2 * PAIR, rows), BF16),
             pltpu.VMEM((DV + ONES, 2 * rows), BF16),
             pltpu.VMEM((2 * parts, 1, rows), F32),
             pltpu.VMEM((2 * parts, DV + ONES, rows), F32),
@@ -538,10 +550,11 @@
             pltpu.VMEM((slots * n_lane, LANES), F32),
             pltpu.VMEM((slots, n_lane, LANES), BF16),
             pltpu.VMEM((slots, n_lane, LANES), BF16),
-            pltpu.VMEM((n_tp, slots, width), BF16),
-            pltpu.VMEM((slots, fe), BF16),
-            pltpu.VMEM((n_tp, slots, width), BF16),
-            pltpu.VMEM((n_tp, slots, width), BF16),
+            pltpu.VMEM((2, n_tp, slots // 2, width), BF16),
+            pltpu.VMEM((n_tp * slots // 2, fe), BF16),
+            pltpu.VMEM((2, n_tp, slots // 2, width), BF16),
+            pltpu.VMEM((2, n_tp, slots // 2, width), BF16),
+            pltpu.VMEM((slots, n_lane, LANES), BF16),
             pltpu.VMEM((slots, n_lane, LANES), BF16),
             pltpu.VMEM((slots, width), BF16),
             pltpu.VMEM((n_tp, tokens, width), BF16),
@@ -551,8 +564,8 @@
             dma((heads,)), dma((parts,)),
             dma((heads,)), dma((n_ep // 2,)), dma((n_ep // 2,)), dma((n_ep // 2,)), dma((n_ep // 2,)),
             dma((parts,)), dma((heads,)),
-            dma((n_tp,)), dma((n_tp,)),
-            dma((n_tp,)), dma((n_tp,)),
+            dma((2, n_tp)), dma((2, n_tp)),
+            dma((2, n_tp)), dma((2, n_tp)),
             dma((n_ep,)), dma((n_ep,)),
             dma((n_tp,)), dma((n_tp,)),
         ],

time: 223 us -> 181 us (0.81)
  the two profiles are of different devices: /device:TPU:33 before, /device:TPU:425 now
where the time goes in v3:
time: 181 us
  Pallas kernels  177 us (98%)
  local copies, waits for them, and re-layouts  3.34 us (2%)
    pallas_call x1, Pallas kernels, local(): pl.pallas_call(functools.partial(kernel, n_ep, n_tp, cap, stages), out_sh...  177 us

profile of v3, /device:TPU:425, one launch (start us, length us, event | category | flops | bytes accessed | tf_op | source)
XLA Modules:
  0.0 180.9 jit_solution(11051477297696531643)
XLA Ops:
  0.6 176.9 %mixer_and_experts.1 = (bf16[64,2048]{1,0:T(8,128)(2,1)}, bf16[64,2048]{1,0:T(8,128)(2,1)}) custom-call(bf16[256,512]{1,0:T(8,128)(2,1)} %q_ref.1, bf16[256,512]{1,0:T(8,128)(2,1)} %k_ref.1, bf16[256,512]{1,0:T(8,128)(2,1)} %v_ref.1, f32[8]{0:T(128)} %lam_ref.1, f32[1,64]{1,0:T(1,128)} %bitcast.13, bf16[64,2048]{1,0:T(8,128)(2,1)} %x_ref.1, ...), custom_call_target="tpu_custom_call" | custom-call | tf_op jit(solution)/shard_map/mixer_and_experts/pallas_call | solution.py:529
  177.5 1.7 copy.17
  179.2 1.7 copy.18

commit v4 on v3

--- a/solution.py
+++ b/solution.py
@@ -286,6 +286,8 @@
     def down(i):
         return lax.rem(tp + n_tp - i, n_tp)
 
+    far_first = sorted(range(1, n_tp), key=lambda i: -min(i, n_tp - i))
+
     def x_copy(half, i):
         block = xrows.at[half, tp]
         return tp_copy(block, block, up(i), x_send.at[half, i], x_recv.at[half, i])
@@ -295,7 +297,7 @@
         unpack_tiles(landed, half * band, n_ep // 2)
         for j in range(n_lane):
             xrows[half, tp, :, j * LANES : (j + 1) * LANES] = wide[pl.ds(j, band, stride=n_lane), :].astype(BF16)
-        for i in range(1, n_tp):
+        for i in far_first:
             x_copy(half, i).start()
 
     def p_copy(half, i):
@@ -317,7 +319,7 @@
         for c0 in range(0, width, cols):
             share = dot(act[...], dw[:, c0 : c0 + cols]).astype(BF16)
             part[half, :, :, c0 : c0 + cols] = share.reshape(n_tp, band, cols)
-        for i in range(1, n_tp):
+        for i in far_first:
             p_copy(half, i).start()
 
     def stage_return(half):
@@ -441,20 +443,24 @@
     each(heads, attends, lambda h: h_arrival(h).wait_recv(), None)
 
     head_rows = h_in[...].astype(F32).reshape(heads * DV, rows).T.astype(BF16)
-    for c0 in range(0, width, step_cols):
-        share = dot(head_rows, ow[:, c0 : c0 + step_cols]).astype(BF16)
-        for d in range(n_tp):
-            mp[d, :, c0 : c0 + step_cols] = share[tokens * d : tokens * (d + 1)]
-
-    def m_copy(i):
-        return tp_copy(mp.at[up(i)], mrecv.at[tp], up(i), m_send.at[i], m_recv.at[i])
-
-    def m_arrival(i):
-        here = mrecv.at[down(i)]
-        return tp_copy(here, here, down(i), m_send.at[i], m_recv.at[i])
-
-    for i in range(1, n_tp):
-        m_copy(i).start()
+    side_cols = width // 2
+    block_cols = min(side_cols, 512)
+
+    def m_copy(i, c):
+        cut = pl.ds(c * side_cols, side_cols)
+        return tp_copy(mp.at[up(i), :, cut], mrecv.at[tp, :, cut], up(i), m_send.at[c, i], m_recv.at[c, i])
+
+    def m_arrival(i, c):
+        here = mrecv.at[down(i), :, pl.ds(c * side_cols, side_cols)]
+        return tp_copy(here, here, down(i), m_send.at[c, i], m_recv.at[c, i])
+
+    for c in (0, 1):
+        for c0 in range(c * side_cols, (c + 1) * side_cols, block_cols):
+            share = dot(head_rows, ow[:, c0 : c0 + block_cols]).astype(BF16)
+            for d in range(n_tp):
+                mp[d, :, c0 : c0 + block_cols] = share[tokens * d : tokens * (d + 1)]
+        for i in far_first:
+            m_copy(i, c).start()
 
     for half in (0, 1):
         over_half(half, lambda d: back_arrival(d).wait_recv())
@@ -472,12 +478,14 @@
     post = lax.rsqrt(jnp.mean(combined * combined, axis=-1, keepdims=True) + POST_EPS)
     eo_ref[...] = (combined * post).astype(BF16)
 
-    for i in range(1, n_tp):
-        m_arrival(i).wait_recv()
-    mixed = mp[tp].astype(F32)
-    for i in range(1, n_tp):
-        mixed = mixed + mrecv[down(i)].astype(F32)
-    mix_ref[...] = mixed.astype(BF16)
+    for c in (0, 1):
+        cut = slice(c * side_cols, (c + 1) * side_cols)
+        for i in range(1, n_tp):
+            m_arrival(i, c).wait_recv()
+        mixed = mp[tp, :, cut].astype(F32)
+        for i in range(1, n_tp):
+            mixed = mixed + mrecv[down(i), :, cut].astype(F32)
+        mix_ref[:, cut] = mixed.astype(BF16)
 
     for half in (0, 1):
         over_half(half, lambda d: out_copy(d).wait_send())
@@ -486,7 +494,8 @@
             x_copy(half, i).wait_send()
             p_copy(half, i).wait_send()
     for i in range(1, n_tp):
-        m_copy(i).wait_send()
+        for c in (0, 1):
+            m_copy(i, c).wait_send()
     each(heads, attends, lambda h: q_copy(h).wait_send(), None)
     each(parts, asks, lambda i: h_copy(i).wait_send(), None)
 
@@ -567,7 +576,7 @@
             dma((2, n_tp)), dma((2, n_tp)),
             dma((2, n_tp)), dma((2, n_tp)),
             dma((n_ep,)), dma((n_ep,)),
-            dma((n_tp,)), dma((n_tp,)),
+            dma((2, n_tp)), dma((2, n_tp)),
         ],
         compiler_params=pltpu.CompilerParams(
             collective_id=0, has_side_effects=True, vmem_limit_bytes=63 * 1024 * 1024

time: 181 us -> 182 us (level)
  the two profiles are of different devices: /device:TPU:425 before, /device:TPU:419 now
where the time goes in v4:
time: 182 us; the launch traced here: 181 us
  Pallas kernels  177 us (97%)
  local copies, waits for them, and re-layouts  3.34 us (2%)
    pallas_call x1, Pallas kernels, local(): pl.pallas_call(functools.partial(kernel, n_ep, n_tp, cap, stages), out_sh...  177 us

profile of v4, /device:TPU:419, one launch (start us, length us, event | category | flops | bytes accessed | tf_op | source)
XLA Modules:
  0.0 181.4 jit_solution(10931519626737489369)
XLA Ops:
  0.6 177.4 %mixer_and_experts.1 = (bf16[64,2048]{1,0:T(8,128)(2,1)}, bf16[64,2048]{1,0:T(8,128)(2,1)}) custom-call(bf16[256,512]{1,0:T(8,128)(2,1)} %q_ref.1, bf16[256,512]{1,0:T(8,128)(2,1)} %k_ref.1, bf16[256,512]{1,0:T(8,128)(2,1)} %v_ref.1, f32[8]{0:T(128)} %lam_ref.1, f32[1,64]{1,0:T(1,128)} %bitcast.13, bf16[64,2048]{1,0:T(8,128)(2,1)} %x_ref.1, ...), custom_call_target="tpu_custom_call" | custom-call | tf_op jit(solution)/shard_map/mixer_and_experts/pallas_call | solution.py:538
  178.1 1.7 copy.17
  179.7 1.7 copy.18
